TPU v7x, 512 devices: a whole 4x8x8 slice. The times are simulated.
512 devices in a mesh: ep: 32 (over z, x), tp: 16 (over y, core).
Axes of the slice: x: 4, y: 8, z: 8, core: 2. Of those that a mesh axis runs over, the one named last changes fastest.
Arguments:
- tokens: bfloat16 [4096, 2048], P('ep'), may hold values from -6 to 6
- routing: int32 [4096, 2], P('ep'), may hold values from 0 to 31, all different within a row; in each aligned block of 128 rows (0 to 127, 128 to 255, ...) at most 14 rows name the same one
- router_weight: bfloat16 [2048, 32], replicated, may hold values from -0.125 to 0.125
- gate_weight: bfloat16 [32, 2048, 2048], P('ep', None, 'tp'), may hold values from -0.125 to 0.125
- up_weight: bfloat16 [32, 2048, 2048], P('ep', None, 'tp'), may hold values from -0.125 to 0.125
- down_weight: bfloat16 [32, 2048, 2048], P('ep', 'tp'), may hold values from -0.125 to 0.125
- cotangent: bfloat16 [4096, 2048], P('ep'), may hold values from -0.796875 to 0.796875
Outputs:
- token_grad: bfloat16 [4096, 2048], P('ep')
- router_grad: float32 [2048, 32], P('tp')
- router_rows: float32 [2048], P('tp')
- gate_grad: bfloat16 [32, 2048, 2048], P('ep', None, 'tp')
- up_grad: bfloat16 [32, 2048, 2048], P('ep', None, 'tp')
- down_grad: bfloat16 [32, 2048, 2048], P('ep', 'tp')
- gate_rows: float32 [32, 2048], P('ep')
- up_rows: float32 [32, 2048], P('ep')
- down_rows: float32 [32, 2048], P('ep', 'tp')
Inputs may be any that keep to these rules, and one draw needn't show every extreme that they name: `routing`: A row's 2 experts differ. Within the rows of one index of ep (128 rows), no expert is named more than 14 times, a bound that some block reaches.
All inputs are finite; a program needn't handle non-finite values.
Results may differ from a plain program's by a relative error of at most 0.01.
Values may be sent and summed in bfloat16 or wider, within the bound.
A program may use at most 64 MiB of HBM per device.

v0:
```python
import jax
import jax.numpy as jnp
from jax import lax
from jax.sharding import PartitionSpec as P


def sent_to_all(shard, axis):
    copies = jnp.broadcast_to(shard, (lax.axis_size(axis), *shard.shape))
    return lax.all_to_all(copies, axis, split_axis=0, concat_axis=0, tiled=True)


def over_copies(shard, axis):
    return sent_to_all(shard, axis).sum(axis=0)


def packed_total(arrays, axis):
    ends = [0]
    for a in arrays:
        ends.append(ends[-1] + a.size)
    running = over_copies(jnp.concatenate([a.ravel() for a in arrays]), axis)
    return tuple((running[b:e].reshape(a.shape) for a, b, e in zip(arrays, ends, ends[1:])))


def sent_together(arrays, axis, split_dim, concat_dim, along):
    columns = [a.reshape(*a.shape[:along], -1) for a in arrays]
    both = jnp.concatenate(columns, axis=along)
    out, at, gathered = (
        lax.all_to_all(both, axis, split_axis=split_dim, concat_axis=concat_dim, tiled=True),
        0,
        [],
    )
    for a, column in zip(arrays, columns):
        slab = out[..., at : at + column.shape[along]]
        gathered.append(slab.reshape(*slab.shape[:along], *a.shape[along:]))
        at += column.shape[along]
    return tuple(gathered)


def expert_backward(rows_in, cots_in, slot_scale, w_gate, w_up, w_down):
    pre_gate = jnp.dot(rows_in, w_gate, preferred_element_type=jnp.float32)
    pre_up = jnp.dot(rows_in, w_up, preferred_element_type=jnp.float32)
    sigmoid_gate = jax.nn.sigmoid(pre_gate)
    hidden = (pre_gate * sigmoid_gate * pre_up).astype(jnp.bfloat16)
    back_proj = lax.dot_general(
        cots_in, w_down, (((1,), (1,)), ((), ())), preferred_element_type=jnp.float32
    )
    gate_term = jnp.sum(hidden.astype(jnp.float32) * back_proj, axis=1)
    scaled = slot_scale * back_proj
    grad_up_pre = (scaled * pre_gate * sigmoid_gate).astype(jnp.bfloat16)
    grad_gate_pre = (
        scaled * pre_up * sigmoid_gate * (1.0 + pre_gate * (1.0 - sigmoid_gate))
    ).astype(jnp.bfloat16)
    weighted = (slot_scale * cots_in.astype(jnp.float32)).astype(jnp.bfloat16)
    contract_rows = (((0,), (0,)), ((), ()))
    grad_down = lax.dot_general(hidden, weighted, contract_rows, preferred_element_type=jnp.float32)
    grad_gate = lax.dot_general(
        rows_in, grad_gate_pre, contract_rows, preferred_element_type=jnp.float32
    )
    grad_up = lax.dot_general(
        rows_in, grad_up_pre, contract_rows, preferred_element_type=jnp.float32
    )
    contract_hidden = (((1,), (1,)), ((), ()))
    partial_value = lax.dot_general(
        grad_gate_pre, w_gate, contract_hidden, preferred_element_type=jnp.float32
    )
    partial_value = partial_value + lax.dot_general(
        grad_up_pre, w_up, contract_hidden, preferred_element_type=jnp.float32
    )
    return (partial_value, gate_term, grad_gate, grad_up, grad_down)


def per_device(tokens, routing, router_weight, gate_weight, up_weight, down_weight, cotangent):
    groups = lax.axis_size("ep")
    shares = lax.axis_size("tp")
    tok_count, model_width = tokens.shape
    top_count = routing.shape[1]
    local_experts = gate_weight.shape[0]
    experts = local_experts * groups
    capacity = 7 * tok_count * top_count // (4 * experts)
    slot_span = groups * capacity
    assigns = tok_count * top_count
    col_width = model_width // shares
    col_start = lax.axis_index("tp") * col_width
    logits = jnp.dot(tokens, router_weight, preferred_element_type=jnp.float32)
    affinity = jax.nn.sigmoid(logits)
    chosen = jnp.take_along_axis(affinity, routing, axis=1)
    total_aff = jnp.sum(chosen, axis=1, keepdims=True)
    weights = chosen / total_aff
    flat_ids = routing.reshape(-1)
    onehot_ids = (flat_ids[:, None] == jnp.arange(experts, dtype=jnp.int32)[None, :]).astype(
        jnp.int32
    )
    position = jnp.sum((jnp.cumsum(onehot_ids, axis=0) - 1) * onehot_ids, axis=1)
    slot_of = flat_ids % local_experts * slot_span + flat_ids // local_experts * capacity + position
    slot_table = jnp.full((local_experts * slot_span,), assigns, jnp.int32)
    slot_table = slot_table.at[slot_of].set(jnp.arange(assigns, dtype=jnp.int32))
    zero_row = jnp.zeros((1, model_width), jnp.bfloat16)
    tok_pad = jnp.concatenate([tokens, zero_row], axis=0)
    cot_pad = jnp.concatenate([cotangent, zero_row], axis=0)
    weight_pad = jnp.concatenate(
        [weights.astype(jnp.bfloat16).reshape(-1), jnp.zeros((1,), jnp.bfloat16)]
    )
    source_tok = slot_table // top_count
    rows_send = tok_pad[source_tok].reshape(local_experts, groups, capacity, model_width)
    cots_send = cot_pad[source_tok].reshape(local_experts, groups, capacity, model_width)
    scale_send = weight_pad[slot_table].reshape(local_experts, groups, capacity)
    rows_recv, cots_recv, scale_recv = (
        lax.all_to_all(rows_send, "ep", split_axis=1, concat_axis=1, tiled=True),
        lax.all_to_all(cots_send, "ep", split_axis=1, concat_axis=1, tiled=True),
        lax.all_to_all(scale_send, "ep", split_axis=1, concat_axis=1, tiled=True),
    )
    partials, gate_terms, gate_grads, up_grads, down_grads = ([], [], [], [], [])
    slot_scale = scale_recv[0].reshape(slot_span).astype(jnp.float32)[:, None]
    result = expert_backward(
        rows_recv[0].reshape(slot_span, model_width),
        cots_recv[0].reshape(slot_span, model_width),
        slot_scale,
        gate_weight[0],
        up_weight[0],
        down_weight[0],
    )
    partials.append(result[0])
    gate_terms.append(result[1])
    gate_grads.append(result[2])
    up_grads.append(result[3])
    down_grads.append(result[4])
    partial_value = jnp.stack(partials)
    gate_term = jnp.stack(gate_terms)
    grad_gate = jnp.stack(gate_grads)
    grad_up = jnp.stack(up_grads)
    grad_down = jnp.stack(down_grads)
    gate_rows, up_rows = packed_total(
        (jnp.sum(grad_gate * grad_gate, axis=2), jnp.sum(grad_up * grad_up, axis=2)), "tp"
    )
    down_rows = jnp.sum(grad_down * grad_down, axis=2)
    summed = lax.psum_scatter(partial_value, "tp", scatter_dimension=2, tiled=True)
    gate_sum = lax.psum(gate_term, "tp")
    back_send = summed.astype(jnp.bfloat16).reshape(local_experts, groups, capacity, col_width)
    gate_send = gate_sum.astype(jnp.bfloat16).reshape(local_experts, groups, capacity)
    back_recv, gate_recv = sent_together((back_send, gate_send), "ep", 1, 1, 3)
    router_cols = lax.dynamic_slice_in_dim(router_weight, col_start, col_width, 0)
    back_flat = back_recv.reshape(local_experts * slot_span, -1)
    back_rows = jnp.sum(
        back_flat[slot_of].astype(jnp.float32).reshape(tok_count, top_count, -1), axis=1
    )
    d_weights = gate_recv.reshape(-1)[slot_of].astype(jnp.float32).reshape(tok_count, top_count)
    d_chosen = (d_weights - jnp.sum(d_weights * weights, axis=1, keepdims=True)) / total_aff
    d_logit = d_chosen * chosen * (1.0 - chosen)
    onehot = (routing[:, :, None] == jnp.arange(experts, dtype=jnp.int32)[None, None, :]).astype(
        jnp.float32
    )
    d_logits = jnp.sum(d_logit[:, :, None] * onehot, axis=1).astype(jnp.bfloat16)
    token_cols = lax.dynamic_slice_in_dim(tokens, col_start, col_width, 1)
    router_part = lax.dot_general(
        token_cols, d_logits, (((0,), (0,)), ((), ())), preferred_element_type=jnp.float32
    )
    router_grad = over_copies(router_part, "ep")
    router_rows = jnp.sum(router_grad * router_grad, axis=1)
    router_back = lax.dot_general(
        d_logits, router_cols, (((1,), (1,)), ((), ())), preferred_element_type=jnp.float32
    )
    token_grad = (back_rows + router_back).astype(jnp.bfloat16)
    token_grad = lax.all_gather(token_grad, "tp", axis=1, tiled=True)
    return (
        token_grad,
        router_grad,
        router_rows,
        grad_gate.astype(jnp.bfloat16),
        grad_up.astype(jnp.bfloat16),
        grad_down.astype(jnp.bfloat16),
        gate_rows,
        up_rows,
        down_rows,
    )


def solution(mesh):
    return jax.shard_map(
        per_device,
        mesh=mesh,
        in_specs=(
            P("ep", None),
            P("ep", None),
            P(),
            P("ep", None, "tp"),
            P("ep", None, "tp"),
            P("ep", "tp", None),
            P("ep", None),
        ),
        out_specs=(
            P("ep", None),
            P("tp", None),
            P("tp"),
            P("ep", None, "tp"),
            P("ep", None, "tp"),
            P("ep", "tp", None),
            P("ep", None),
            P("ep", None),
            P("ep", "tp"),
        ),
        check_vma=False,
    )
```

profile of v0, /device:TPU:1, one launch (start us, length us, event | category | flops | bytes accessed | tf_op | source)
XLA Modules:
  0.0 301.1 jit_solution(10308237477314463072)
XLA Ops:
  7.2 0.7 bitcast_or_fusion
  7.9 0.7 broadcast_multiply_fusion
  8.6 0.8 copy.91
  9.4 0.1 eq.44
  9.5 0.1 eq.40
  9.8 0.1 mul.106
  10.1 0.1 reshape.215
  10.2 1.4 fusion.5
  11.6 2.0 gather_fusion.5
  14.0 0.2 convert_element_type.88
  14.1 0.6 reduce-window.6
  14.7 0.2 slice_reduce_fusion.1
  15.1 1.4 scatter_custom_fusion
  16.5 3.2 %gather_fusion = bf16[448]{0:T(512)(128)(2,1)S(1)} fusion(bf16[257]{0:T(512)(128)(2,1)S(1)} %pad_maximum_fusion.1, s32[1024]{0:T(1024)S(1)} %get-tuple-element.82), kind=kCustom, calls=%fused_computation | custom fusion | bytes 3584 | tf_op jit(solution)/shard_map/gather | solution.py:106
  19.7 0.7 reshape.237
  20.4 13.7 %all-to-all-start = ((bf16[1,32,14]{2,0,1:T(2,128)(2,1)}), bf16[1,32,14]{2,0,1:T(2,128)(2,1)S(1)}, u32[]{:S(2)}, u32[]{:S(2)}) async-start(bf16[1,32,14]{2,0,1:T(2,128)(2,1)} %reshape.237), calls=%async_computation | async-start | bytes 32768 | tf_op jit(solution)/shard_map/all_to_all | solution.py:110
  34.2 2.5 gather_fusion.2
  36.7 1.6 reshape.167
  38.3 4.4 %all-to-all-done = bf16[1,32,14]{2,0,1:T(2,128)(2,1)S(1)} async-done(((bf16[1,32,14]{2,0,1:T(2,128)(2,1)}), bf16[1,32,14]{2,0,1:T(2,128)(2,1)S(1)}, u32[]{:S(2)}, u32[]{:S(2)}) %all-to-all-start) | async-done | bytes 928 | tf_op jit(solution)/shard_map/all_to_all | solution.py:110
  42.7 4.8 %all-to-all-start.2 = ((bf16[1,32,14,2048]{3,2,0,1:T(8,128)(2,1)}), bf16[1,32,14,2048]{3,2,0,1:T(8,128)(2,1)S(1)}, u32[]{:S(2)}, u32[]{:S(2)}) async-start(bf16[1,32,14,2048]{3,2,0,1:T(8,128)(2,1)} %bitcast.81), calls=%async_computation.2 | async-start | bytes 4194304 | tf_op jit(solution)/shard_map/all_to_all | solution.py:108
  47.5 1.1 concatenate.16
  48.6 3.2 %gather_fusion.1 = bf16[448,2048]{1,0:T(8,128)(2,1)} fusion(bf16[129,2048]{1,0:T(8,128)(2,1)S(1)} %concatenate.16, s32[1024]{0:T(1024)S(1)} %get-tuple-element.81), kind=kCustom, calls=%fused_computation.1 | custom fusion | bytes 3671808 | tf_op jit(solution)/shard_map/gather | solution.py:105
  51.8 3.6 %reshape.166 = bf16[1,32,14,2048]{3,2,1,0:T(8,128)(2,1)} reshape(bf16[448,2048]{1,0:T(8,128)(2,1)} %gather_fusion.1) | data formatting | bytes 3670016 | tf_op jit(solution)/shard_map/reshape | solution.py:105
  55.4 40.0 %all-to-all-done.2 = bf16[1,32,14,2048]{3,2,0,1:T(8,128)(2,1)S(1)} async-done(((bf16[1,32,14,2048]{3,2,0,1:T(8,128)(2,1)}), bf16[1,32,14,2048]{3,2,0,1:T(8,128)(2,1)S(1)}, u32[]{:S(2)}, u32[]{:S(2)}) %all-to-all-start.2) | async-done | bytes 1835040 | tf_op jit(solution)/shard_map/all_to_all | solution.py:108
  95.5 1.3 copy-done.1
  96.8 6.8 %all-to-all-start.1 = ((bf16[1,32,14,2048]{3,2,0,1:T(8,128)(2,1)}), bf16[1,32,14,2048]{3,2,0,1:T(8,128)(2,1)}, u32[]{:S(2)}, u32[]{:S(2)}) async-start(bf16[1,32,14,2048]{3,2,0,1:T(8,128)(2,1)} %bitcast.80), calls=%async_computation.1 | async-start | bytes 4194304 | tf_op jit(solution)/shard_map/all_to_all | solution.py:109
  103.8 2.6 reshape_squeeze.8
  106.4 0.6 fusion.8
  107.1 0.4 copy-done.3
  107.5 0.6 fusion.11
  108.1 42.1 %all-to-all-done.1 = bf16[1,32,14,2048]{3,2,0,1:T(8,128)(2,1)} async-done(((bf16[1,32,14,2048]{3,2,0,1:T(8,128)(2,1)}), bf16[1,32,14,2048]{3,2,0,1:T(8,128)(2,1)}, u32[]{:S(2)}, u32[]{:S(2)}) %all-to-all-start.1) | async-done | bytes 1835040 | tf_op jit(solution)/shard_map/all_to_all | solution.py:109
  150.2 3.7 %reshape_squeeze.7 = bf16[448,2048]{1,0:T(8,128)(2,1)} reshape(bf16[1,32,14,2048]{3,2,0,1:T(8,128)(2,1)} %all-to-all-done.1) | data formatting | bytes 3670016 | tf_op jit(solution)/shard_map/reshape;squeeze | solution.py:116
  153.9 2.9 multiply_reduce_fusion.3
  156.8 0.6 fusion.6
  157.4 2.5 add_bitcast_fusion
  159.9 47.2 %psum.7 = bf16[1,448]{1,0:T(2,128)(2,1)S(1)} all-reduce(f32[1,448]{1,0:T(1,128)S(1)} %bitcast.90), channel_id=1, replica_groups=mesh['ep'=32,'tp'=16] {'tp'}, use_global_device_ids=true, to_apply=%region_7.8 | all-reduce | flops 448 | bytes 2688 | tf_op jit(solution)/shard_map/psum | solution.py:137
  207.2 0.3 reshape_reshape.8
  207.5 1.3 multiply_reduce_fusion.2
  208.8 15.8 %reduce-scatter.2.cloned.1.call-done = f32[1,448,128]{2,1,0:T(8,128)} async-done(((f32[1,448,2048]{2,1,0:T(8,128)}), f32[1,448,128]{2,1,0:T(8,128)}) %reduce-scatter.2.cloned.1.call-update) | async-done | bytes 229392 | tf_op jit(solution)/shard_map/reduce_scatter | solution.py:136
  224.5 1.0 convert_element_type.94
  225.6 1.0 reshape.250
  226.6 8.8 %all-to-all-start.3 = ((bf16[32,2,903]{2,1,0:T(2,128)(2,1)}), bf16[32,2,903]{2,1,0:T(2,128)(2,1)S(1)}, u32[]{:S(2)}, u32[]{:S(2)}) async-start(bf16[32,2,903]{2,1,0:T(2,128)(2,1)} %reshape.250), calls=%async_computation.4 | async-start | bytes 262144 | tf_op jit(solution)/shard_map/all_to_all | solution.py:28
  235.4 0.5 multiply_reduce_fusion.1
  235.9 2.0 copy.102
  237.9 1.0 copy.103
  238.9 5.8 %all-to-all-done.3 = bf16[32,2,903]{2,1,0:T(2,128)(2,1)S(1)} async-done(((bf16[32,2,903]{2,1,0:T(2,128)(2,1)}), bf16[32,2,903]{2,1,0:T(2,128)(2,1)S(1)}, u32[]{:S(2)}, u32[]{:S(2)}) %all-to-all-start.3) | async-done | bytes 115616 | tf_op jit(solution)/shard_map/all_to_all | solution.py:28
  244.7 0.9 broadcast_in_dim.36
  245.6 9.5 %all-to-all-start.5 = ((f32[16,1,4096]{2,1,0:T(1,128)}), f32[16,1,4096]{2,1,0:T(1,128)S(1)}, u32[]{:S(2)}, u32[]{:S(2)}) async-start(f32[16,1,4096]{2,1,0:T(1,128)} %broadcast_in_dim.36), calls=%async_computation.6 | async-start | bytes 524288 | tf_op jit(solution)/shard_map/all_to_all | solution.py:9
  255.1 1.2 reshape.251
  256.3 0.2 slice_reduce_fusion
  256.6 1.9 gather_fusion.4
  258.8 0.9 fusion.17
  259.7 7.0 %all-to-all-done.5 = f32[16,1,4096]{2,1,0:T(1,128)S(1)} async-done(((f32[16,1,4096]{2,1,0:T(1,128)}), f32[16,1,4096]{2,1,0:T(1,128)S(1)}, u32[]{:S(2)}, u32[]{:S(2)}) %all-to-all-start.5) | async-done | bytes 262176 | tf_op jit(solution)/shard_map/all_to_all | solution.py:9
  266.7 0.9 broadcast_in_dim.18
  267.5 3.9 %all-to-all-start.4 = ((f32[32,128,32]{1,2,0:T(8,128)}), f32[32,128,32]{1,2,0:T(8,128)S(1)}, u32[]{:S(2)}, u32[]{:S(2)}) async-start(f32[32,128,32]{1,2,0:T(8,128)} %broadcast_in_dim.18), calls=%async_computation.5 | async-start | bytes 1048576 | tf_op jit(solution)/shard_map/all_to_all | solution.py:9
  271.4 2.8 multiply_reduce_fusion
  274.2 0.2 reduce_sum.123
  274.4 0.6 fusion.32
  275.1 0.9 gather_fusion.3
  275.9 0.2 convert_reduce_fusion
  276.1 0.9 fusion.2
  277.0 15.9 %all_gather.3 = bf16[128,2048]{1,0:T(8,128)(2,1)S(1)} all-gather(bf16[128,128]{1,0:T(8,128)(2,1)S(1)} %fusion.2), channel_id=1, replica_groups=mesh['ep'=32,'tp'=16] {'tp'}, dimensions={1}, use_global_device_ids=true | all-gather | bytes 557056 | tf_op jit(solution)/shard_map/all_gather | solution.py:163
  293.0 0.5 multiply_reduce_fusion.4
  293.5 0.8 copy.110
  (54 shorter events, 1.7 us)
Async XLA Ops:
  7.2 99.2 %copy-start = (bf16[1,2048,128]{2,1,0:T(8,128)(2,1)S(1)}, bf16[1,2048,128]{2,1,0:T(8,128)(2,1)}, u32[]{:S(2)}) copy-start(bf16[1,2048,128]{2,1,0:T(8,128)(2,1)} %param.10) | copy-start | bytes 1572868
  11.6 2.2 copy-start.9
  13.6 20.6 %copy-start.2 = (bf16[128,2048]{1,0:T(8,128)(2,1)S(1)}, bf16[128,2048]{1,0:T(8,128)(2,1)}, u32[]{:S(2)}) copy-start(bf16[128,2048]{1,0:T(8,128)(2,1)} %param.7) | copy-start | bytes 1572868
  20.4 22.2 %all-to-all-start = ((bf16[1,32,14]{2,0,1:T(2,128)(2,1)}), bf16[1,32,14]{2,0,1:T(2,128)(2,1)S(1)}, u32[]{:S(2)}, u32[]{:S(2)}) async-start(bf16[1,32,14]{2,0,1:T(2,128)(2,1)} %reshape.237), calls=%async_computation | async-start | bytes 32768 | tf_op jit(solution)/shard_map/all_to_all | solution.py:110
  42.7 52.8 %all-to-all-start.2 = ((bf16[1,32,14,2048]{3,2,0,1:T(8,128)(2,1)}), bf16[1,32,14,2048]{3,2,0,1:T(8,128)(2,1)S(1)}, u32[]{:S(2)}, u32[]{:S(2)}) async-start(bf16[1,32,14,2048]{3,2,0,1:T(8,128)(2,1)} %bitcast.81), calls=%async_computation.2 | async-start | bytes 4194304 | tf_op jit(solution)/shard_map/all_to_all | solution.py:108
  95.4 1.3 copy-start.1
  96.8 53.4 %all-to-all-start.1 = ((bf16[1,32,14,2048]{3,2,0,1:T(8,128)(2,1)}), bf16[1,32,14,2048]{3,2,0,1:T(8,128)(2,1)}, u32[]{:S(2)}, u32[]{:S(2)}) async-start(bf16[1,32,14,2048]{3,2,0,1:T(8,128)(2,1)} %bitcast.80), calls=%async_computation.1 | async-start | bytes 4194304 | tf_op jit(solution)/shard_map/all_to_all | solution.py:109
  103.6 120.9 %reduce-scatter.2.cloned.1.call-start = ((), (), s32[]{:S(2)}) async-start(), calls=%async_computation.7 | async-start | bytes 3899392 | tf_op jit(solution)/shard_map/reduce_scatter | solution.py:136
  106.4 1.0 copy-start.3
  156.8 0.6 copy-start.6
  159.9 47.6 %copy-start.7 = (bf16[448,128]{1,0:T(8,128)(2,1)S(1)}, bf16[448,128]{1,0:T(8,128)(2,1)}, u32[]{:S(2)}) copy-start(bf16[448,128]{1,0:T(8,128)(2,1)} %copy-done.6) | copy-start | bytes 344068
  226.6 18.1 %all-to-all-start.3 = ((bf16[32,2,903]{2,1,0:T(2,128)(2,1)}), bf16[32,2,903]{2,1,0:T(2,128)(2,1)S(1)}, u32[]{:S(2)}, u32[]{:S(2)}) async-start(bf16[32,2,903]{2,1,0:T(2,128)(2,1)} %reshape.250), calls=%async_computation.4 | async-start | bytes 262144 | tf_op jit(solution)/shard_map/all_to_all | solution.py:28
  238.9 32.5 %copy-start.4 = (bf16[448,2048]{1,0:T(8,128)(2,1)S(1)}, bf16[448,2048]{1,0:T(8,128)(2,1)}, u32[]{:S(2)}) copy-start(bf16[448,2048]{1,0:T(8,128)(2,1)} %reshape_squeeze.7) | copy-start | bytes 5505028
  244.7 0.9 copy-start.5
  245.6 21.1 %all-to-all-start.5 = ((f32[16,1,4096]{2,1,0:T(1,128)}), f32[16,1,4096]{2,1,0:T(1,128)S(1)}, u32[]{:S(2)}, u32[]{:S(2)}) async-start(f32[16,1,4096]{2,1,0:T(1,128)} %broadcast_in_dim.36), calls=%async_computation.6 | async-start | bytes 524288 | tf_op jit(solution)/shard_map/all_to_all | solution.py:9
  267.5 25.4 %all-to-all-start.4 = ((f32[32,128,32]{1,2,0:T(8,128)}), f32[32,128,32]{1,2,0:T(8,128)S(1)}, u32[]{:S(2)}, u32[]{:S(2)}) async-start(f32[32,128,32]{1,2,0:T(8,128)} %broadcast_in_dim.18), calls=%async_computation.5 | async-start | bytes 1048576 | tf_op jit(solution)/shard_map/all_to_all | solution.py:9
  293.0 1.3 copy-start.8
Sparse Core Ops, SparseCore 0:
  160.0 64.4 reduce-scatter.1
where the time goes:
time: 302 us; the launch traced here: 301 us
  waiting for transfers between devices  115 us (38%)
  blocking collectives  63.1 us (21%)
  starting transfers between devices  47.6 us (16%)
  local copies, waits for them, and re-layouts  41.7 us (14%)
  matrix products  15 us (5%)
  between operations  14.5 us (5%)
  other arithmetic  4.28 us (1%)
    psum x1, blocking collectives, per_device(): gate_sum = lax.psum(gate_term, 'tp')  47.2 us
    all_to_all x1, waiting for transfers between devices, per_device(): lax.all_to_all(cots_send, 'ep', split_axis=1, concat_axis=1, tiled=True)  42.1 us
    all_to_all x1, waiting for transfers between devices, per_device(): lax.all_to_all(rows_send, 'ep', split_axis=1, concat_axis=1, tiled=True)  40 us
    all_gather x1, blocking collectives, per_device(): token_grad = lax.all_gather(token_grad, 'tp', axis=1, tiled=True)  15.9 us
    reduce_scatter x1, waiting for transfers between devices, per_device(): lax.psum_scatter(partial_value, 'tp', scatter_dimension=2, tiled=True)  15.8 us
    all_to_all x1, starting transfers between devices, per_device(): lax.all_to_all(scale_send, 'ep', split_axis=1, concat_axis=1, tiled=True)  13.7 us
    all_to_all x2, starting transfers between devices, sent_to_all(): return lax.all_to_all(copies, axis, split_axis=0, concat_axis=0, tiled=True)  13.4 us
    all_to_all x1, starting transfers between devices, sent_together(): lax.all_to_all(both, axis, split_axis=split_dim, concat_axis=concat_dim,...  8.79 us
  transfers between devices with their start and end apart: 7, of which 6 were waited for; matrix products, arithmetic and copies ran while one was open for 10% of the time, Pallas kernels for 0%

commit v1 on v0

v1 whole, which is shorter than its diff:
```python
import functools

import jax
import jax.numpy as jnp
from jax import lax
from jax.experimental import pallas as pl
from jax.experimental.pallas import tpu as pltpu
from jax.sharding import PartitionSpec as P

BF = jnp.bfloat16
F32 = jnp.float32
CW = 128
SUB = 112
HI = lax.Precision.HIGHEST
NN = ((1,), (0,))
NT = ((1,), (1,))
TN = ((0,), (0,))


def dot(a, b, dims=NN, precision=None):
    return lax.dot_general(a, b, (dims, ((), ())), precision=precision, preferred_element_type=F32)


def iota(shape, dim):
    return lax.broadcasted_iota(jnp.int32, shape, dim)


def one_hot(mask, dtype=BF):
    return jnp.where(mask, 1.0, 0.0).astype(dtype)


def kernel(
    cfg,
    routing, rw, tok_h, cot_h, gw_h, uw_h, dw_h,
    tg_o, rg_o, rr_o, gg_o, ug_o, dg_o, rows_o, drow_o,
    tok_v, cot_v, w_own, w_par, dn_v,
    sel_v, cmp_v, sx, rx, sz, rz_, xa, za, wcol, acc_gu, acc_b,
    hid_v, gp_own, gp_par, tm_v, part_v, rs_s, rs_r, ret_s, ret_r,
    g_s, g_r, gf_r, zr_r, xr_s, xr_r, row_v, rowd_r, rowy_s, rowy_r, rowf_s, tg_r,
    ld_sem, a_send, a_recv, y_send, y_recv, d_send, d_recv, w_send, w_recv, gp_send, gp_recv,
    g_send, g_recv, gf_send, gf_recv, rs_send, rs_recv, ret_send, ret_recv,
    z_send, z_recv, x_send, x_recv, rd_send, rd_recv, ry_send, ry_recv, rf_send, rf_recv,
    t_send, t_recv, td_send, td_recv,
):
    EP, NX, NY, T, D, CAP, PC = cfg
    NZ = EP // NX
    TP = 2 * NY
    H = NY // 2
    ROWS = EP * CAP
    SLOTS = EP * PC
    NS = ROWS // SUB
    shift = PC.bit_length() - 1
    inv = 65536 // CAP + 1
    ep = lax.axis_index("ep")
    tp = lax.axis_index("tp")
    y = lax.div(tp, 2)
    c = lax.rem(tp, 2)
    zc = lax.div(ep, NX)
    xc = lax.rem(ep, NX)
    partner = {"tp": y * 2 + (1 - c)}

    def ydev(off):
        return {"tp": lax.rem(y + off + NY, NY) * 2 + c}

    def remote(src, dst, ss, rs, dev):
        return pltpu.make_async_remote_copy(
            src_ref=src, dst_ref=dst, send_sem=ss, recv_sem=rs, device_id=dev,
            device_id_type=pl.DeviceIdType.MESH,
        )

    def each(lo, hi, body):
        def step(i, carry):
            body(i)
            return carry

        lax.fori_loop(lo, hi, step, 0)

    cols = pl.ds(pl.multiple_of(tp * CW, CW), CW)
    ld_tok = pltpu.make_async_copy(tok_h, tok_v, ld_sem.at[0])
    ld_cot = pltpu.make_async_copy(cot_h.at[:, cols], cot_v, ld_sem.at[1])
    ld_g = pltpu.make_async_copy(gw_h.at[0], w_own.at[0], ld_sem.at[2])
    ld_u = pltpu.make_async_copy(uw_h.at[0], w_own.at[1], ld_sem.at[3])
    ld_d = pltpu.make_async_copy(dw_h.at[0], dn_v, ld_sem.at[4])
    for cp in (ld_tok, ld_cot, ld_g, ld_u, ld_d):
        cp.start()
    barrier = pltpu.get_barrier_semaphore()

    def greet_ep(d):
        pl.semaphore_signal(barrier, inc=1, device_id={"ep": lax.rem(ep + d, EP)},
                            device_id_type=pl.DeviceIdType.MESH)

    def greet_tp(d):
        pl.semaphore_signal(barrier, inc=1, device_id={"tp": lax.rem(tp + d, TP)},
                            device_id_type=pl.DeviceIdType.MESH)

    each(1, EP, greet_ep)
    each(1, TP, greet_tp)

    e_lane = iota((T, EP), 1)
    chosen_mask = (e_lane == routing[:, 0:1]) | (e_lane == routing[:, 1:2])
    hit = one_hot(chosen_mask)
    earlier = one_hot(iota((T, T), 1) < iota((T, T), 0))
    count = dot(earlier, hit).astype(BF)
    spread = one_hot((iota((EP, SLOTS), 1) >> shift) == iota((EP, SLOTS), 0))
    slot_lane = (iota((T, SLOTS), 1) & (PC - 1)).astype(F32)
    sel = jnp.where((dot(count, spread) == slot_lane) & (dot(hit, spread) > 0.5), 1.0, 0.0)
    sel_v[...] = sel.astype(BF)
    lane_of = one_hot((iota((SLOTS, CW), 0) & (PC - 1)) == iota((SLOTS, CW), 1))
    tail = one_hot(
        ((iota((SLOTS, EP), 0) >> shift) == iota((SLOTS, EP), 1))
        & ((iota((SLOTS, EP), 0) & (PC - 1)) == CAP)
    )
    row_id = iota((ROWS, SLOTS), 0)
    row_src = (row_id * inv) >> 16
    cmp_v[...] = one_hot(iota((ROWS, SLOTS), 1) == row_id + (PC - CAP) * row_src)

    ld_tok.wait()
    affinity = jax.nn.sigmoid(dot(tok_v[...], rw[...]))
    hit32 = hit.astype(F32)
    chosen = affinity * hit32
    total = jnp.sum(chosen, axis=1, keepdims=True)
    weights = chosen / total
    wx = dot(weights.astype(BF), spread)
    slot_w = jnp.sum(sel * wx, axis=0, keepdims=True)
    w_rows = dot((spread.astype(F32) * slot_w).astype(BF), lane_of)
    tok_cols = tok_v[:, cols]
    ld_cot.wait()
    send_x = dot(sel.astype(BF), tok_cols, TN) + dot(tail, w_rows.astype(BF))
    sx[...] = send_x.astype(BF).reshape(EP, PC, CW)
    sz[...] = dot(sel.astype(BF), cot_v[...], TN).astype(BF).reshape(EP, PC, CW)

    pl.semaphore_wait(barrier, EP - 1 + TP - 1)

    def a2a(part, src, dst, peer):
        return remote(src.at[peer], dst.at[ep], a_send.at[part, peer], a_recv.at[part, ep], {"ep": peer})

    def a2a_wait(part, src, dst, peer):
        return remote(src.at[peer], dst.at[peer], a_send.at[part, peer], a_recv.at[part, peer], {"ep": peer})

    def peer_of(d):
        return lax.rem(ep + d, EP)

    each(1, EP, lambda d: a2a(0, sx, rx, peer_of(d)).start())
    each(1, EP, lambda d: a2a(1, sz, rz_, peer_of(d)).start())
    rx[ep] = sx[ep]
    rz_[ep] = sz[ep]
    ld_g.wait()
    ld_u.wait()
    ld_d.wait()
    cp_w = remote(w_own, w_par, w_send, w_recv, partner)
    cp_w.start()

    bufs = (xa, za)

    def hop(way, step, part, src):
        blk = bufs[part].at[src, c]
        return remote(blk, blk, y_send.at[way, step - 1, part], y_recv.at[way, step - 1, part],
                      ydev(1 if way == 0 else -1))

    def cross(part, src):
        blk = bufs[part].at[src, c]
        return remote(blk, blk, d_send.at[part, src], d_recv.at[part, src], partner)

    def cross_wait(part, src):
        blk = bufs[part].at[src, 1 - c]
        remote(blk, blk, d_send.at[part, src], d_recv.at[part, src], partner).wait_recv()

    each(1, EP, lambda d: a2a_wait(0, sx, rx, peer_of(d)).wait_recv())
    rx_all = rx[...].reshape(SLOTS, CW)
    xa[y, c] = dot(cmp_v[...], rx_all).astype(BF)
    hop(0, 1, 0, y).start()
    if H > 1:
        hop(1, 1, 0, y).start()
    cross(0, y).start()
    each(1, EP, lambda d: a2a_wait(1, sz, rz_, peer_of(d)).wait_recv())
    za[y, c] = dot(cmp_v[...], rz_[...].reshape(SLOTS, CW)).astype(BF)
    if H > 1:
        hop(0, 1, 1, y).start()
    hop(1, 1, 1, y).start()
    cross(1, y).start()

    pick = one_hot(
        iota((ROWS, SLOTS), 1) == (row_src * PC + CAP)
    )
    w_sel = dot(pick, rx_all)
    r2 = iota((ROWS, CW), 0)
    r2_pos = r2 - ((r2 * inv) >> 16) * CAP
    w_masked = jnp.where(r2_pos == iota((ROWS, CW), 1), w_sel, 0.0)
    wcol[...] = jnp.broadcast_to(jnp.sum(w_masked, axis=1, keepdims=True), (ROWS, CW))

    acc_gu[...] = jnp.zeros_like(acc_gu)
    acc_b[...] = jnp.zeros_like(acc_b)

    def chunk_ds(src):
        return pl.ds(pl.multiple_of(src * 2 * CW, 2 * CW), 2 * CW)

    def forward_chunk(src):
        cross_wait(0, src)
        xs = jnp.concatenate([xa[src, 0], xa[src, 1]], axis=1)
        ds = chunk_ds(src)
        wgu = jnp.concatenate([w_own[0, ds, :], w_own[1, ds, :]], axis=1)
        acc_gu[...] += dot(xs, wgu)
        cross_wait(1, src)
        zs = jnp.concatenate([za[src, 0], za[src, 1]], axis=1)
        acc_b[...] += dot(zs, dn_v[:, ds], NT)

    def at(off):
        return lax.rem(y + off + NY, NY)

    def parts_of(way, step):
        return (0, 1) if step < H else ((0,) if way == 0 else (1,))

    each(0, 1, lambda i: forward_chunk(at(i)))
    for s in range(1, H + 1):
        for part in (0, 1):
            for way in (0, 1):
                if part not in parts_of(way, s):
                    continue
                src = at(-s if way == 0 else s)
                hop(way, s, part, src).wait_recv()
                if s < H and part in parts_of(way, s + 1):
                    hop(way, s + 1, part, src).start()
                cross(part, src).start()
        if s < H:
            each(0, 2, lambda i, s=s: forward_chunk(at((2 * i - 1) * s)))
    each(0, 1, lambda i: forward_chunk(at(H + i)))

    RB = 32

    def pointwise(i):
        ds = pl.ds(pl.multiple_of(i * RB, RB), RB)
        pg = acc_gu[ds, :CW]
        pu = acc_gu[ds, CW:]
        bk = acc_b[ds, :]
        s = jax.nn.sigmoid(pg)
        hid = (pg * s * pu).astype(BF)
        hid_v[ds, :] = hid
        term = jnp.sum(hid.astype(F32) * bk, axis=1, keepdims=True)
        rr = iota((RB, CW), 0) + i * RB
        pos = rr - ((rr * inv) >> 16) * CAP
        tm_v[ds, :] = jnp.where(pos == iota((RB, CW), 1), term, 0.0)
        sc = wcol[ds, :] * bk
        gp_own[ds, :CW] = (sc * pu * s * (1.0 + pg * (1.0 - s))).astype(BF)
        gp_own[ds, CW:] = (sc * pg * s).astype(BF)

    each(0, ROWS // RB, pointwise)
    cp_gp = remote(gp_own, gp_par, gp_send, gp_recv, partner)
    cp_gp.start()

    block_of = one_hot(((iota((EP, ROWS), 1) * inv) >> 16) == iota((EP, ROWS), 0), F32)
    g_s[...] = dot(block_of, tm_v[...], NN, HI).reshape(EP, 1, CW)
    g_r[ep] = g_s[ep]

    def g_copy(peer, slot):
        return remote(g_s.at[peer], g_r.at[slot], g_send.at[peer], g_recv.at[slot], {"ep": peer})

    each(1, EP, lambda d: g_copy(peer_of(d), ep).start())

    cp_w.wait_recv()
    cp_gp.wait_recv()

    def partial_for(off):
        base = pl.multiple_of(at(off) * 2 * CW + c * CW, CW)
        ds = pl.ds(base, CW)
        own = jnp.concatenate([w_own[0, ds, :], w_own[1, ds, :]], axis=1)
        par = jnp.concatenate([w_par[0, ds, :], w_par[1, ds, :]], axis=1)
        return dot(gp_own[...], own, NT) + dot(gp_par[...], par, NT)

    def rs(way, step, i):
        ds = pl.ds(i * SUB, SUB)
        return remote(rs_s.at[way, step - 1, ds], rs_r.at[way, step - 1, ds],
                      rs_send.at[way, step - 1, i], rs_recv.at[way, step - 1, i],
                      ydev(1 if way == 0 else -1))

    def subs(way, step):
        if step > 1:
            return tuple(range(NS))
        return tuple(range(NS // 2, NS)) if way == 0 else tuple(range(NS // 2))

    first = partial_for(H)
    for way in (0, 1):
        half = pl.ds(subs(way, 1)[0] * SUB, ROWS // 2)
        lo = subs(way, 1)[0] * SUB
        rs_s[way, 0, half] = first[lo:lo + ROWS // 2].astype(BF)
        for i in subs(way, 1):
            rs(way, 1, i).start()

    def own_parts(step):
        part_v[0] = partial_for(H - step + 1)
        part_v[1] = partial_for(-(H - step + 1))

    def rs_step(step):
        have = [(i, w) for i in range(NS) for w in (0, 1)]
        have.sort(key=lambda t: (t[0] in subs(t[1], step - 1)))
        for i, w in have:
            ds = pl.ds(i * SUB, SUB)
            val = part_v[w, ds, :]
            if i in subs(w, step - 1):
                rs(w, step - 1, i).wait_recv()
                val = val + rs_r[w, step - 2, ds, :].astype(F32)
            rs_s[w, step - 1, ds, :] = val.astype(BF)
            rs(w, step, i).start()

    ones = jnp.ones((8, 2 * CW), BF)
    drow_o[...] = jnp.zeros_like(drow_o)

    def grads(src):
        ds = chunk_ds(src)
        xs = jnp.concatenate([xa[src, 0], xa[src, 1]], axis=1)
        gu = dot(xs, gp_own[...], TN)
        gg_o[ds, :] = gu[:, :CW].astype(BF)
        ug_o[ds, :] = gu[:, CW:].astype(BF)
        sq = (gu * gu).astype(BF)
        for k in (0, 1):
            tot = dot(ones[:, :CW], sq[:, k * CW:(k + 1) * CW], NT)
            row_v[k, pl.ds(src * 2, 1)] = tot[0:1, :CW].reshape(1, 1, CW)
            row_v[k, pl.ds(src * 2 + 1, 1)] = tot[0:1, CW:].reshape(1, 1, CW)
        scale = wcol[...]
        w0 = (scale * za[src, 0].astype(F32)).astype(BF)
        w1 = (scale * za[src, 1].astype(F32)).astype(BF)
        dgr = dot(hid_v[...], jnp.concatenate([w0, w1], axis=1), TN)
        dg_o[:, ds] = dgr.astype(BF)
        drow_o[...] += dot(ones, (dgr * dgr).astype(BF), NT)

    per = -(-NY // H)

    def some_grads(k):
        each(k * per, min(NY, (k + 1) * per), grads)

    own_parts(2)
    some_grads(0)
    rs_step(2)

    each(1, EP, lambda d: g_copy(peer_of(d), peer_of(d)).wait_recv())
    lane_t = one_hot((iota((CW, SLOTS), 1) & (PC - 1)) == iota((CW, SLOTS), 0), F32)
    spread32 = one_hot((iota((EP, SLOTS), 1) >> shift) == iota((EP, SLOTS), 0), F32)
    g_flat = jnp.sum(dot(g_r[...].reshape(EP, CW), lane_t, NN, HI) * spread32, axis=0, keepdims=True)
    gf_r[tp] = g_flat

    def gf(peer, slot):
        return remote(gf_r.at[tp], gf_r.at[slot], gf_send.at[peer], gf_recv.at[slot], {"tp": peer})

    def gf_wait(peer):
        remote(gf_r.at[peer], gf_r.at[peer], gf_send.at[peer], gf_recv.at[peer], {"tp": peer}).wait_recv()

    def tpeer(d):
        return lax.rem(tp + d, TP)

    each(1, TP, lambda d: gf(tpeer(d), tp).start())

    def rs_rest(step):
        own_parts(step)
        some_grads(step - 2)
        rs_step(step)

    for step in range(3, H + 1):
        rs_rest(step)
        if step == 3:
            gather_terms = True
    each(1, TP, lambda d: gf_wait(tpeer(d)))
    g_tot = gf_r[0]
    for j in range(1, TP):
        g_tot = g_tot + gf_r[j]
    g_tot = g_tot.astype(BF).astype(F32)
    d_w = dot((sel_v[...].astype(F32) * g_tot).astype(BF), one_hot(
        (iota((SLOTS, EP), 0) >> shift) == iota((SLOTS, EP), 1)))
    d_chosen = (d_w - jnp.sum(d_w * weights, axis=1, keepdims=True)) / total
    d_logits = (d_chosen * chosen * (1.0 - affinity) * hit32).astype(BF)
    tok_c = tok_v[:, cols]
    zr_r[zc] = dot(d_logits, tok_c, TN)

    def zdev(off):
        return {"ep": lax.rem(zc + off, NZ) * NX + xc}

    def zsend(d):
        return remote(zr_r.at[zc], zr_r.at[zc], z_send.at[d - 1], z_recv.at[zc], zdev(d))

    def zwait(d):
        k = lax.rem(zc + d, NZ)
        remote(zr_r.at[k], zr_r.at[k], z_send.at[d - 1], z_recv.at[k], zdev(d)).wait_recv()

    each(1, NZ, lambda d: zsend(d).start())

    some_grads(H - 1)
    own = partial_for(0)

    hb = D // CW

    def rowd(k):
        return remote(row_v.at[k], rowd_r, rd_send, rd_recv, partner)

    rowd(1 - c).start()

    rd_wait = rowd(1 - c)

    out_rows = []
    for i in range(NS):
        ds = pl.ds(i * SUB, SUB)
        val = own[i * SUB:(i + 1) * SUB]
        for w in (0, 1):
            rs(w, H, i).wait_recv()
            val = val + rs_r[w, H - 1, ds, :].astype(F32)
        out_rows.append(val.astype(BF))
    slot_grad = jnp.concatenate(out_rows, axis=0)
    ret_s[...] = dot(cmp_v[...], slot_grad, TN).astype(BF).reshape(EP, PC, CW)

    def ret(peer, slot):
        return remote(ret_s.at[peer], ret_r.at[slot], ret_send.at[peer], ret_recv.at[slot], {"ep": peer})

    each(1, EP, lambda d: ret(peer_of(d), ep).start())
    ret_r[ep] = ret_s[ep]

    rd_wait.wait_recv()
    rowy_r[y] = row_v[c] + rowd_r[...]

    def ry(d):
        return remote(rowy_r.at[y], rowy_r.at[y], ry_send.at[d - 1], ry_recv.at[y], ydev(d))

    def ry_wait(d):
        k = at(d)
        remote(rowy_r.at[k], rowy_r.at[k], ry_send.at[d - 1], ry_recv.at[k], ydev(d)).wait_recv()

    each(1, NY, lambda d: ry(d).start())

    each(1, NZ, lambda d: zwait(d))
    z_tot = zr_r[0]
    for j in range(1, NZ):
        z_tot = z_tot + zr_r[j]
    xr_r[xc] = z_tot

    def xdev(off):
        return {"ep": zc * NX + lax.rem(xc + off, NX)}

    def xsend(d):
        return remote(xr_r.at[xc], xr_r.at[xc], x_send.at[d - 1], x_recv.at[xc], xdev(d))

    def xwait(d):
        k = lax.rem(xc + d, NX)
        remote(xr_r.at[k], xr_r.at[k], x_send.at[d - 1], x_recv.at[k], xdev(d)).wait_recv()

    each(1, NX, lambda d: xsend(d).start())
    router_back = dot(d_logits, rw[cols, :], NT)

    each(1, EP, lambda d: ret(peer_of(d), peer_of(d)).wait_recv())
    back = dot(sel_v[...], ret_r[...].reshape(SLOTS, CW))
    tg_r[y, c] = (back + router_back).astype(BF)

    def tg(d):
        blk = tg_r.at[y, c]
        return remote(blk, blk, t_send.at[d - 1], t_recv.at[y], ydev(d))

    def tg_wait(d):
        blk = tg_r.at[at(d), c]
        remote(blk, blk, t_send.at[d - 1], t_recv.at[at(d)], ydev(d)).wait_recv()

    def tgd(src):
        blk = tg_r.at[src, c]
        return remote(blk, blk, td_send.at[src], td_recv.at[src], partner)

    def tgd_wait(src):
        blk = tg_r.at[src, 1 - c]
        remote(blk, blk, td_send.at[src], td_recv.at[src], partner).wait_recv()

    each(1, NY, lambda d: tg(d).start())
    tgd(y).start()

    each(1, NY, lambda d: ry_wait(d))
    r_tot = rowy_r[0]
    for j in range(1, NY):
        r_tot = r_tot + rowy_r[j]
    rowf_s[c] = r_tot
    rf = remote(rowf_s.at[c], rowf_s.at[c], rf_send, rf_recv, partner)
    rf.start()
    each(1, NX, lambda d: xwait(d))
    x_tot = xr_r[0]
    for j in range(1, NX):
        x_tot = x_tot + xr_r[j]
    rg_o[...] = x_tot
    rr_o[...] = jnp.sum(x_tot * x_tot, axis=0, keepdims=True)

    def arrive(d):
        tg_wait(d)
        tgd(at(d)).start()

    each(1, NY, arrive)
    remote(rowf_s.at[1 - c], rowf_s.at[1 - c], rf_send, rf_recv, partner).wait_recv()
    rows_o[...] = rowf_s[...]
    each(0, NY, tgd_wait)
    for j in range(NY):
        for k in (0, 1):
            tg_o[:, (2 * j + k) * CW:(2 * j + k + 1) * CW] = tg_r[j, k]

    def drain_ep(d):
        p = peer_of(d)
        a2a(0, sx, rx, p).wait_send()
        a2a(1, sz, rz_, p).wait_send()
        g_copy(p, ep).wait_send()
        ret(p, ep).wait_send()

    each(1, EP, drain_ep)
    each(1, TP, lambda d: gf(tpeer(d), tp).wait_send())
    each(1, NZ, lambda d: zsend(d).wait_send())
    each(1, NX, lambda d: xsend(d).wait_send())

    def drain_y(d):
        ry(d).wait_send()
        tg(d).wait_send()

    each(1, NY, drain_y)

    def drain_d(s):
        cross(0, s).wait_send()
        cross(1, s).wait_send()
        tgd(s).wait_send()

    each(0, NY, drain_d)
    for s in range(1, H + 1):
        for way in (0, 1):
            for part in parts_of(way, s):
                hop(way, s, part, y).wait_send()
            for i in subs(way, s):
                rs(way, s, i).wait_send()
    cp_w.wait_send()
    cp_gp.wait_send()
    rd_wait.wait_send()
    rf.wait_send()


def build(ep, nx, ny, tok, width, cap):
    pc = 1
    while pc <= cap:
        pc *= 2
    rows, slots, tp, half = ep * cap, ep * pc, 2 * ny, ny // 2
    ns = rows // SUB
    hb = width // CW
    nz = ep // nx
    cfg = (ep, nx, ny, tok, width, cap, pc)
    v = pltpu.VMEM
    dma = pltpu.SemaphoreType.DMA
    scratch = [
        v((tok, width), BF), v((tok, CW), BF), v((2, width, CW), BF), v((2, width, CW), BF), v((CW, width), BF),
        v((tok, slots), BF), v((rows, slots), BF),
        v((ep, pc, CW), BF), v((ep, pc, CW), BF), v((ep, pc, CW), BF), v((ep, pc, CW), BF),
        v((ny, 2, rows, CW), BF), v((ny, 2, rows, CW), BF),
        v((rows, CW), F32), v((rows, 2 * CW), F32), v((rows, CW), F32),
        v((rows, CW), BF), v((rows, 2 * CW), BF), v((rows, 2 * CW), BF), v((rows, CW), F32),
        v((2, rows, CW), F32), v((2, half, rows, CW), BF), v((2, half, rows, CW), BF),
        v((ep, pc, CW), BF), v((ep, pc, CW), BF),
        v((ep, 1, CW), F32), v((ep, 1, CW), F32), v((tp, 1, slots), F32),
        v((nz, ep, CW), F32), v((ep, CW), F32), v((nx, ep, CW), F32),
        v((2, hb, 1, CW), F32), v((hb, 1, CW), F32), v((hb, 1, CW), F32), v((ny, hb, 1, CW), F32),
        v((2, hb, 1, CW), F32), v((ny, 2, tok, CW), BF),
        dma((5,)), dma((2, ep)), dma((2, ep)), dma((2, half, 2)), dma((2, half, 2)),
        dma((2, ny)), dma((2, ny)), dma, dma, dma, dma,
        dma((ep,)), dma((ep,)), dma((tp,)), dma((tp,)), dma((2, half, ns)), dma((2, half, ns)),
        dma((ep,)), dma((ep,)), dma((nz,)), dma((nz,)), dma((nx,)), dma((nx,)), dma, dma,
        dma((ny,)), dma((ny,)), dma, dma, dma((ny,)), dma((ny,)), dma((ny,)), dma((ny,)),
    ]
    out_shape = (
        jax.ShapeDtypeStruct((tok, width), BF),
        jax.ShapeDtypeStruct((ep, CW), F32),
        jax.ShapeDtypeStruct((1, CW), F32),
        jax.ShapeDtypeStruct((width, CW), BF),
        jax.ShapeDtypeStruct((width, CW), BF),
        jax.ShapeDtypeStruct((CW, width), BF),
        jax.ShapeDtypeStruct((2, hb, 1, CW), F32),
        jax.ShapeDtypeStruct((8, CW), F32),
    )
    vm = pl.BlockSpec(memory_space=pltpu.VMEM)
    hb_ = pl.BlockSpec(memory_space=pl.ANY)
    call = pl.pallas_call(
        functools.partial(kernel, cfg),
        out_shape=out_shape,
        in_specs=[vm, vm, hb_, hb_, hb_, hb_, hb_],
        out_specs=tuple([vm] * 8),
        scratch_shapes=scratch,
        compiler_params=pltpu.CompilerParams(
            collective_id=0, has_side_effects=True, vmem_limit_bytes=56 * 1024 * 1024
        ),
        name="experts_backward",
    )

    def per_device(tokens, routing, router_weight, gate_weight, up_weight, down_weight, cotangent):
        tg, rg, rr, gg, ug, dg, rows2, drow = call(
            routing, router_weight, tokens, cotangent, gate_weight, up_weight, down_weight
        )
        return (
            tg, rg.T, rr.reshape(CW), gg[None], ug[None], dg[None],
            rows2[0].reshape(1, width), rows2[1].reshape(1, width), drow[0:1],
        )

    return per_device


SPECS_IN = (
    P("ep", None), P("ep", None), P(), P("ep", None, "tp"), P("ep", None, "tp"), P("ep", "tp", None), P("ep", None),
)
SPECS_OUT = (
    P("ep", None), P("tp", None), P("tp"), P("ep", None, "tp"), P("ep", None, "tp"), P("ep", "tp", None),
    P("ep", None), P("ep", None), P("ep", "tp"),
)


def solution(mesh):
    ep, tp = mesh.shape["ep"], mesh.shape["tp"]
    body = build(ep, 4, tp // 2, 128, CW * tp, 14)
    return jax.shard_map(body, mesh=mesh, in_specs=SPECS_IN, out_specs=SPECS_OUT, check_vma=False)
```

time: 302 us -> 100 us (0.33)
  waiting for transfers between devices: 115 us -> 0 us
  Pallas kernels: 0 us -> 87.6 us
  blocking collectives: 63.1 us -> 0 us
  starting transfers between devices: 47.6 us -> 0 us
  local copies, waits for them, and re-layouts: 41.7 us -> 11.5 us
  matrix products: 15 us -> 0 us
  between operations: 14.5 us -> 0.67 us
  other arithmetic: 4.28 us -> 0 us
    all_to_all x6 -> x0, waiting for transfers between devices: 99.3 us -> none  [the longest x1 42.1 us: per_device(): lax.all_to_all(cots_send, 'ep', split_axis=1, concat_axis=1, tiled=True)]
    pallas_call x0 -> x1, Pallas kernels: none -> 87.6 us  [per_device(): call(routing, router_weight, tokens, cotangent, gate_weight, up_weight, d...]
    all_to_all x6 -> x0, starting transfers between devices: 47.5 us -> none  [the longest x1 13.7 us: per_device(): lax.all_to_all(scale_send, 'ep', split_axis=1, concat_axis=1, tiled=True)]
    psum x1 -> x0, blocking collectives: 47.2 us -> none  [per_device(): gate_sum = lax.psum(gate_term, 'tp')]
    all_gather x1 -> x0, blocking collectives: 15.9 us -> none  [per_device(): token_grad = lax.all_gather(token_grad, 'tp', axis=1, tiled=True)]
    reduce_scatter x1 -> x0, waiting for transfers between devices: 15.8 us -> none  [per_device(): lax.psum_scatter(partial_value, 'tp', scatter_dimension=2, tiled=True)]
    dot_general x11 -> x0, matrix products: 15 us -> none  [the longest x1 2.89 us: expert_backward(): lax.dot_general(cots_in, w_down, (((1,), (1,)), ((), ())), preferred_elem...]
    gather x10 -> x0, local copies, waits for them, and re-layouts: 14.1 us -> none  [the longest x1 3.23 us: per_device(): cot_pad[source_tok].reshape(local_experts, groups, capacity, model_width)]
  transfers between devices with their start and end apart: 7 -> 0, of which waited for: 6 -> 0; matrix products, arithmetic and copies ran while one was open for 10% -> 0% of each run, Pallas kernels for 0% -> 0%
where the time goes in v1:
time: 100 us; the launch traced here: 99.8 us
  Pallas kernels  87.6 us (88%)
  local copies, waits for them, and re-layouts  11.5 us (12%)
    pallas_call x1, Pallas kernels, per_device(): call(routing, router_weight, tokens, cotangent, gate_weight, up_weight, d...  87.6 us
    unnamed x20, local copies, waits for them, and re-layouts  9.7 us

profile of v1, /device:TPU:1, one launch (start us, length us, event | category | flops | bytes accessed | tf_op | source)
XLA Modules:
  0.0 99.8 jit_solution(17417953687330652006)
XLA Ops:
  0.6 1.4 %copy.16.routing = s32[128,2]{1,0:T(8,128)} copy(s32[128,2]{0,1:T(2,128)} %param.8) | data formatting | bytes 2048 | tf_op args[1]
  2.1 1.9 %copy.17.rw = bf16[2048,32]{1,0:T(8,128)(2,1)} copy(bf16[2048,32]{0,1:T(8,128)(2,1)} %param.9) | data formatting | bytes 262144 | tf_op args[2]
  4.0 87.6 %experts_backward.1 = (bf16[128,2048]{1,0:T(8,128)(2,1)}, f32[32,128]{1,0:T(8,128)}, f32[1,128]{1,0:T(1,128)}, bf16[2048,128]{1,0:T(8,128)(2,1)}, bf16[2048,128]...) custom-call(s32[128,2]{1,0:T(8,128)} %copy.16.routing, ...), custom_call_target="tpu_custom_call" | custom-call | tf_op jit(solution)/shard_map/experts_backward/pallas_call | solution.py:584
  91.6 0.0 copy-start.4
  91.6 1.2 %slice.11 = f32[1,128]{1,0:T(1,128)} slice(f32[8,128]{1,0:T(8,128)} %get-tuple-element.24), slice={[0:1], [0:128]} | slice | bytes 1024 | tf_op jit(solution)/shard_map/slice | solution.py:589
  92.8 0.0 copy-done.4
  92.8 0.6 slice_bitcast_fusion
  93.4 0.0 copy-start.3
  93.4 0.0 copy-start.2
  93.4 1.9 %copy.24 = bf16[128,2048]{1,0:T(8,128)(2,1)} copy(bf16[128,2048]{1,0:T(8,128)(2,1)} %get-tuple-element.36) | data formatting | bytes 1048576
  95.4 0.0 copy-done.3
  95.4 0.0 copy-start.5
  95.4 0.6 copy.25
  96.0 0.1 copy-done.5
  96.0 0.5 copy.26
  96.5 0.0 copy-done.2
  96.5 0.0 copy-start.1
  96.5 0.8 copy.27
  97.3 0.4 copy-done.1
  97.8 0.0 copy-start
  97.8 0.8 copy.28
  98.6 0.4 copy-done
  99.0 0.8 copy.29
Async XLA Ops:
  91.6 1.2 %copy-start.4 = (f32[2,16,1,128]{3,2,1,0:T(1,128)S(1)}, f32[2,16,1,128]{3,2,1,0:T(1,128)}, u32[]{:S(2)}) copy-start(f32[2,16,1,128]{3,2,1,0:T(1,128)} %get-tuple-element.23) | copy-start | bytes 49156
  93.4 1.9 %copy-start.3 = (f32[32,128]{1,0:T(8,128)S(1)}, f32[32,128]{1,0:T(8,128)}, u32[]{:S(2)}) copy-start(f32[32,128]{1,0:T(8,128)} %get-tuple-element.18) | copy-start | bytes 49156
  93.4 3.1 %copy-start.2 = (bf16[2048,128]{1,0:T(8,128)(2,1)S(1)}, bf16[2048,128]{1,0:T(8,128)(2,1)}, u32[]{:S(2)}) copy-start(bf16[2048,128]{1,0:T(8,128)(2,1)} %get-tuple-element.20) | copy-start | bytes 1572868
  95.4 0.7 copy-start.5
  96.5 1.2 %copy-start.1 = (bf16[2048,128]{1,0:T(8,128)(2,1)S(1)}, bf16[2048,128]{1,0:T(8,128)(2,1)}, u32[]{:S(2)}) copy-start(bf16[2048,128]{1,0:T(8,128)(2,1)} %get-tuple-element.21) | copy-start | bytes 1572868
  97.8 1.2 %copy-start = (bf16[128,2048]{1,0:T(8,128)(2,1)S(1)}, bf16[128,2048]{1,0:T(8,128)(2,1)}, u32[]{:S(2)}) copy-start(bf16[128,2048]{1,0:T(8,128)(2,1)} %get-tuple-element.22) | copy-start | bytes 1572868

commit v2 on v1

v2 whole, which is shorter than its diff:
```python
import functools

import jax
import jax.numpy as jnp
from jax import lax
from jax.experimental import pallas as pl
from jax.experimental.pallas import tpu as pltpu
from jax.sharding import PartitionSpec as P

BF = jnp.bfloat16
F32 = jnp.float32
CW = 128
SUB = 112
VMEM_MB = 24
HI = lax.Precision.HIGHEST
NN = ((1,), (0,))
NT = ((1,), (1,))
TN = ((0,), (0,))


def dot(a, b, dims=NN, precision=None):
    return lax.dot_general(a, b, (dims, ((), ())), precision=precision, preferred_element_type=F32)


def iota(shape, dim):
    return lax.broadcasted_iota(jnp.int32, shape, dim)


def one_hot(mask, dtype=BF):
    return jnp.where(mask, 1.0, 0.0).astype(dtype)


def kernel(
    cfg,
    rt_h, rw_h, tok_h, cot_h, gw_h, uw_h, dw_h,
    tg_r, rg_o, rr_o, gg_o, ug_o, dg_o, rowf_s, drow_o,
    rt_v, rw_v, tok_v, cot_v, w_own, w_par, dn_v,
    sel_v, cmp_v, a_s, a_r, xa, za, wcol, acc_gu, acc_b,
    hid_v, gp_own, gp_par, tm_v, part_v, rs_s, rs_r, ret_s, ret_r,
    g_s, g_r, gf_r, zr_r, xr_r, row_v, rowd_r, rowy_r,
    ld_sem, a_send, a_recv, y_send, y_recv, d_send, d_recv, w_send, w_recv, gp_send, gp_recv,
    g_send, g_recv, gf_send, gf_recv, rs_send, rs_recv, ret_send, ret_recv,
    z_send, z_recv, x_send, x_recv, rd_send, rd_recv, ry_send, ry_recv, rf_send, rf_recv,
    t_send, t_recv, td_send, td_recv,
):
    EP, NX, NY, T, D, CAP, PC = cfg
    cur = [None]

    def mark(n):
        if cur[0] is not None:
            cur[0].__exit__(None, None, None)
        cur[0] = None
        if n:
            cur[0] = jax.named_scope(n)
            cur[0].__enter__()

    NZ = EP // NX
    TP = 2 * NY
    H = NY // 2
    ROWS = EP * CAP
    SLOTS = EP * PC
    NS = ROWS // SUB
    shift = PC.bit_length() - 1
    inv = 65536 // CAP + 1
    ep = lax.axis_index("ep")
    tp = lax.axis_index("tp")
    y = lax.div(tp, 2)
    c = lax.rem(tp, 2)
    zc = lax.div(ep, NX)
    xc = lax.rem(ep, NX)
    partner = {"tp": y * 2 + (1 - c)}

    def ydev(off):
        return {"tp": lax.rem(y + off + NY, NY) * 2 + c}

    def remote(src, dst, ss, rs, dev):
        return pltpu.make_async_remote_copy(
            src_ref=src, dst_ref=dst, send_sem=ss, recv_sem=rs, device_id=dev,
            device_id_type=pl.DeviceIdType.MESH,
        )

    def each(lo, hi, body):
        def step(i, carry):
            body(i)
            return carry

        lax.fori_loop(lo, hi, step, 0)

    mark('load')
    barrier = pltpu.get_barrier_semaphore()

    xs_of = [lax.rem(xc + NX // 2 + (j + 1) // 2 * (1 - 2 * (j % 2)), NX) for j in range(NX)]

    def y_order(k):
        return H + lax.div(k + 1, 2) * (1 - 2 * lax.rem(k, 2))

    def each_peer(body):
        def plane(k):
            dz = NZ // 2 + lax.div(k + 1, 2) * (1 - 2 * lax.rem(k, 2))
            base = lax.rem(zc + dz, NZ) * NX
            for x in xs_of:
                body(base + x)

        each(0, NZ - 1, plane)
        for x in xs_of[:-1]:
            body(zc * NX + x)

    def settle(ref, sem):
        pltpu.make_async_copy(ref, ref, sem).wait()

    def greet_ep(peer):
        pl.semaphore_signal(barrier, inc=1, device_id={"ep": peer}, device_id_type=pl.DeviceIdType.MESH)

    def greet_tp(d):
        pl.semaphore_signal(barrier, inc=1, device_id={"tp": lax.rem(tp + d, TP)},
                            device_id_type=pl.DeviceIdType.MESH)

    each_peer(greet_ep)
    each(1, TP, greet_tp)
    ld_rt = pltpu.make_async_copy(rt_h, rt_v, ld_sem.at[5])
    ld_rw = pltpu.make_async_copy(rw_h, rw_v, ld_sem.at[6])
    ld_tok = pltpu.make_async_copy(tok_h, tok_v, ld_sem.at[0])
    ld_cot = pltpu.make_async_copy(cot_h, cot_v, ld_sem.at[1])
    ld_g = pltpu.make_async_copy(gw_h.at[0], w_own.at[0], ld_sem.at[2])
    ld_u = pltpu.make_async_copy(uw_h.at[0], w_own.at[1], ld_sem.at[3])
    ld_d = pltpu.make_async_copy(dw_h.at[0], dn_v, ld_sem.at[4])
    for cp in (ld_rt, ld_tok, ld_rw, ld_cot, ld_g, ld_u, ld_d):
        cp.start()

    mark('tables')
    ld_rt.wait()
    e_row = iota((EP, T), 0)
    hit_t = one_hot((e_row == rt_v[0:1, :]) | (e_row == rt_v[1:2, :]))
    hit = dot(hit_t, one_hot(iota((EP, EP), 0) == iota((EP, EP), 1)), TN).astype(BF)
    earlier = one_hot(iota((T, T), 1) < iota((T, T), 0))
    count = dot(earlier, hit).astype(BF)
    spread = one_hot((iota((EP, SLOTS), 1) >> shift) == iota((EP, SLOTS), 0))
    slot_lane = (iota((T, SLOTS), 1) & (PC - 1)).astype(F32)
    sel = jnp.where((dot(count, spread) == slot_lane) & (dot(hit, spread) > 0.5), 1.0, 0.0)
    sel_v[...] = sel.astype(BF)
    lane_of = one_hot((iota((SLOTS, CW), 0) & (PC - 1)) == iota((SLOTS, CW), 1))
    tail = one_hot(
        ((iota((SLOTS, EP), 0) >> shift) == iota((SLOTS, EP), 1))
        & ((iota((SLOTS, EP), 0) & (PC - 1)) == CAP)
    )
    row_id = iota((ROWS, SLOTS), 0)
    row_src = (row_id * inv) >> 16
    cmp_v[...] = one_hot(iota((ROWS, SLOTS), 1) == row_id + (PC - CAP) * row_src)

    ld_tok.wait()
    ld_rw.wait()
    affinity = jax.nn.sigmoid(dot(tok_v[...], rw_v[...], NT))
    hit32 = hit.astype(F32)
    chosen = affinity * hit32
    total = jnp.sum(chosen, axis=1, keepdims=True)
    weights = chosen / total
    wx = dot(weights.astype(BF), spread)
    slot_w = jnp.sum(sel * wx, axis=0, keepdims=True)
    w_rows = dot((spread.astype(F32) * slot_w).astype(BF), lane_of)
    sel_b = sel.astype(BF)

    def at(off):
        return lax.rem(y + off + NY, NY)

    def col_ds(chip):
        return pl.ds(pl.multiple_of((chip * 2 + c) * CW, CW), CW)

    cols = col_ds(y)
    extra = ((0, y), (1, y), (0, at(H)), (1, at(H)), (0, at(H - 1)), (1, at(1 - H)))
    ld_cot.wait()

    def fill(k):
        kind, chip = extra[k]
        val = dot(sel_b, (tok_v if kind == 0 else cot_v)[:, col_ds(chip)], TN)
        if k == 0:
            val = val + dot(tail, w_rows.astype(BF))
        a_s[k] = val.astype(BF).reshape(EP, PC, CW)
        a_r[k, ep] = a_s[k, ep]

    for k in range(6):
        fill(k)
    mark('barrier')
    pl.semaphore_wait(barrier, EP - 1 + TP - 1)

    mark('a2a_issue')

    def a2a(k, peer):
        return remote(a_s.at[k, peer], a_r.at[k, ep], a_send.at[k], a_recv.at[k], {"ep": peer})

    each_peer(lambda p: a2a(0, p).start())
    each_peer(lambda p: a2a(1, p).start())
    for k in range(2, 6):
        each_peer(lambda p, k=k: a2a(k, p).start())
    ld_g.wait()
    ld_u.wait()
    ld_d.wait()
    cp_w = remote(w_own, w_par, w_send, w_recv, partner)
    cp_w.start()

    bufs = (xa, za)

    def hop(way, step, part, src):
        blk = bufs[part].at[src, c]
        return remote(blk, blk, y_send, y_recv.at[way, step - 1, part],
                      ydev(1 if way == 0 else -1))

    def cross(part, src):
        blk = bufs[part].at[src, c]
        return remote(blk, blk, d_send, d_recv.at[part, src], partner)

    def cross_wait(part, src):
        blk = bufs[part].at[src, 1 - c]
        remote(blk, blk, d_send, d_recv.at[part, src], partner).wait_recv()

    def parts_of(way, step):
        return (0, 1) if step < H - 1 else ((0,) if way == 0 else (1,))

    def take(k):
        kind, chip = extra[k]
        settle(a_r.at[k, pl.ds(0, EP - 1)], a_recv.at[k])
        bufs[kind][chip, c] = dot(cmp_v[...], a_r[k].reshape(SLOTS, CW)).astype(BF)
        cross(kind, chip).start()

    for k in (0, 1):
        mark(f'a2a_wait{k}')
        take(k)
        for way in (0, 1):
            if k in parts_of(way, 1):
                hop(way, 1, k, y).start()
    rx_all = a_r[0].reshape(SLOTS, CW)

    mark('wcol')
    pick = one_hot(
        iota((ROWS, SLOTS), 1) == (row_src * PC + CAP)
    )
    w_sel = dot(pick, rx_all)
    r2 = iota((ROWS, CW), 0)
    r2_pos = r2 - ((r2 * inv) >> 16) * CAP
    w_masked = jnp.where(r2_pos == iota((ROWS, CW), 1), w_sel, 0.0)
    wcol[...] = jnp.broadcast_to(jnp.sum(w_masked, axis=1, keepdims=True), (ROWS, CW))

    acc_gu[...] = jnp.zeros_like(acc_gu)
    acc_b[...] = jnp.zeros_like(acc_b)

    def chunk_ds(src):
        return pl.ds(pl.multiple_of(src * 2 * CW, 2 * CW), 2 * CW)

    def forward_chunk(src):
        cross_wait(0, src)
        xs = jnp.concatenate([xa[src, 0], xa[src, 1]], axis=1)
        ds = chunk_ds(src)
        wgu = jnp.concatenate([w_own[0, ds, :], w_own[1, ds, :]], axis=1)
        acc_gu[...] += dot(xs, wgu)
        cross_wait(1, src)
        zs = jnp.concatenate([za[src, 0], za[src, 1]], axis=1)
        acc_b[...] += dot(zs, dn_v[:, ds], NT)

    mark('fwd0')
    each(0, 1, lambda i: forward_chunk(at(i)))
    for s in range(1, H):
        mark(f'gather{s}')
        for part in (0, 1):
            for way in (0, 1):
                if part not in parts_of(way, s):
                    continue
                src = at(-s if way == 0 else s)
                hop(way, s, part, src).wait_recv()
                if s < H - 1 and part in parts_of(way, s + 1):
                    hop(way, s + 1, part, src).start()
                cross(part, src).start()
        mark(f'fwd{s}')
        if s < H - 1:
            each(0, 2, lambda i, s=s: forward_chunk(at((2 * i - 1) * s)))
        if s == max(1, H - 2):
            mark('extra')
            take(2)
            take(3)
            each(0, 1, lambda i: forward_chunk(at(H + i)))
            take(4)
            take(5)
    mark('fwdL')
    each(0, 2, lambda i: forward_chunk(at((2 * i - 1) * (H - 1))))

    mark('pointwise')
    RB = 32 if ROWS % 64 == 0 and (ROWS // 2) % 32 == 0 else 16

    def pointwise(i):
        ds = pl.ds(pl.multiple_of(i * RB, RB), RB)
        pg = acc_gu[ds, :CW]
        pu = acc_gu[ds, CW:]
        bk = acc_b[ds, :]
        s = jax.nn.sigmoid(pg)
        hid = (pg * s * pu).astype(BF)
        hid_v[ds, :] = hid
        term = jnp.sum(hid.astype(F32) * bk, axis=1, keepdims=True)
        rr = iota((RB, CW), 0) + i * RB
        pos = rr - ((rr * inv) >> 16) * CAP
        tm_v[ds, :] = jnp.where(pos == iota((RB, CW), 1), term, 0.0)
        sc = wcol[ds, :] * bk
        gp_own[ds, :CW] = (sc * pu * s * (1.0 + pg * (1.0 - s))).astype(BF)
        gp_own[ds, CW:] = (sc * pg * s).astype(BF)

    HR = ROWS // 2

    def cp_gp(h):
        ds = pl.ds(h * HR, HR)
        return remote(gp_own.at[ds], gp_par.at[ds], gp_send.at[h], gp_recv.at[h], partner)

    for h in (0, 1):
        each(h * (HR // RB), (h + 1) * (HR // RB), pointwise)
        cp_gp(h).start()

    mark('gpwait')
    def weight_rows(w_v, off):
        ds = pl.ds(pl.multiple_of(at(off) * 2 * CW + c * CW, CW), CW)
        return jnp.concatenate([w_v[0, ds, :], w_v[1, ds, :]], axis=1)

    def partial_for(off):
        return dot(gp_own[...], weight_rows(w_own, off), NT) + dot(gp_par[...], weight_rows(w_par, off), NT)

    def rs(way, step, i):
        ds = pl.ds(i * SUB, SUB)
        return remote(rs_s.at[way * H + step - 1, ds], rs_r.at[way * H + step - 1, ds],
                      rs_send, rs_recv.at[way, step - 1, i],
                      ydev(1 if way == 0 else -1))

    def subs(way, step):
        if step > 1:
            return tuple(range(NS))
        return tuple(range(NS // 2, NS)) if way == 0 else tuple(range(NS // 2))

    own_first = dot(gp_own[...], weight_rows(w_own, H), NT)
    cp_w.wait_recv()
    for h in (0, 1):
        way = 1 - h
        ds = pl.ds(h * HR, HR)
        cp_gp(h).wait_recv()
        val = own_first[h * HR:(h + 1) * HR] + dot(gp_par[ds, :], weight_rows(w_par, H), NT)
        rs_s[way * H, ds] = val.astype(BF)
        for i in subs(way, 1):
            rs(way, 1, i).start()

    def own_parts(step):
        part_v[0] = partial_for(H - step + 1)
        part_v[1] = partial_for(-(H - step + 1))

    def rs_step(step):
        have = [(i, w) for i in range(NS) for w in (0, 1)]
        have.sort(key=lambda t: (t[0] in subs(t[1], step - 1)))
        for i, w in have:
            ds = pl.ds(i * SUB, SUB)
            val = part_v[w, ds, :]
            if i in subs(w, step - 1):
                rs(w, step - 1, i).wait_recv()
                val = val + rs_r[w * H + step - 2, ds, :].astype(F32)
            rs_s[w * H + step - 1, ds, :] = val.astype(BF)
            rs(w, step, i).start()

    mark('gterm')
    block_of = one_hot(((iota((EP, ROWS), 1) * inv) >> 16) == iota((EP, ROWS), 0), F32)
    g_s[...] = dot(block_of, tm_v[...], NN, HI).reshape(EP, 1, CW)
    g_r[ep] = g_s[ep]

    def g_copy(peer, slot):
        return remote(g_s.at[peer], g_r.at[slot], g_send, g_recv, {"ep": peer})

    each_peer(lambda p: g_copy(p, ep).start())

    ones = jnp.ones((8, 2 * CW), BF)

    def grads(src):
        ds = chunk_ds(src)
        xs = jnp.concatenate([xa[src, 0], xa[src, 1]], axis=1)
        gu = dot(xs, gp_own[...], TN)
        gg_o[ds, :] = gu[:, :CW].astype(BF)
        ug_o[ds, :] = gu[:, CW:].astype(BF)
        sq = (gu * gu).astype(BF)
        for k in (0, 1):
            tot = dot(ones[:, :CW], sq[:, k * CW:(k + 1) * CW], NT)
            row_v[k, pl.ds(src * 2, 1)] = tot[0:1, :CW].reshape(1, 1, CW)
            row_v[k, pl.ds(src * 2 + 1, 1)] = tot[0:1, CW:].reshape(1, 1, CW)

    def down_grads(src):
        ds = chunk_ds(src)
        scale = wcol[...]
        w0 = (scale * za[src, 0].astype(F32)).astype(BF)
        w1 = (scale * za[src, 1].astype(F32)).astype(BF)
        dgr = dot(hid_v[...], jnp.concatenate([w0, w1], axis=1), TN)
        dg_o[:, ds] = dgr.astype(BF)
        drow_o[...] += dot(ones, (dgr * dgr).astype(BF), NT)[0:1]

    def flatten_terms():
        mark('gflat')
        settle(g_r.at[pl.ds(0, EP - 1)], g_recv)
        lane_t = one_hot((iota((CW, SLOTS), 1) & (PC - 1)) == iota((CW, SLOTS), 0), F32)
        spread32 = one_hot((iota((EP, SLOTS), 1) >> shift) == iota((EP, SLOTS), 0), F32)
        g_flat = jnp.sum(dot(g_r[...].reshape(EP, CW), lane_t, NN, HI) * spread32, axis=0, keepdims=True)
        gf_r[tp] = g_flat

        def gf(peer, slot):
            return remote(gf_r.at[tp], gf_r.at[slot], gf_send, gf_recv, {"tp": peer})

        def tpeer(d):
            return lax.rem(tp + d, TP)

        each(1, TP, lambda d: gf(tpeer(d), tp).start())

    mark('own2')
    own_parts(2)
    mark('rs2')
    rs_step(2)
    done = 0
    for step in range(3, H + 1):
        mark(f'own{step}')
        own_parts(step)
        each(done, done + 1, grads)
        done += 1
        mark(f'rs{step}')
        rs_step(step)
        if step == 3:
            flatten_terms()
    if H < 3:
        flatten_terms()

    mark('rsfinal')
    own = partial_for(0)
    BPS = SUB // CAP

    def ret(peer, slot):
        return remote(ret_s.at[peer], ret_r.at[slot], ret_send, ret_recv, {"ep": peer})

    for i in range(NS):
        ds = pl.ds(i * SUB, SUB)
        val = own[i * SUB:(i + 1) * SUB]
        for w in (0, 1):
            rs(w, H, i).wait_recv()
            val = val + rs_r[w * H + H - 1, ds, :].astype(F32)
        spread_rows = cmp_v[ds, i * BPS * PC:(i + 1) * BPS * PC]
        ret_s[i * BPS:(i + 1) * BPS] = dot(spread_rows, val.astype(BF), TN).astype(BF).reshape(BPS, PC, CW)

        def send_back(b):
            @pl.when(b != ep)
            def _():
                ret(b, ep).start()

        each(i * BPS, (i + 1) * BPS, send_back)
    ret_r[ep] = ret_s[ep]

    mark('router')
    settle(gf_r.at[pl.ds(0, TP - 1)], gf_recv)
    g_tot = gf_r[0]
    for j in range(1, TP):
        g_tot = g_tot + gf_r[j]
    g_tot = g_tot.astype(BF).astype(F32)
    d_w = dot((sel_v[...].astype(F32) * g_tot).astype(BF), one_hot(
        (iota((SLOTS, EP), 0) >> shift) == iota((SLOTS, EP), 1)))
    d_chosen = (d_w - jnp.sum(d_w * weights, axis=1, keepdims=True)) / total
    d_logits = (d_chosen * chosen * (1.0 - affinity) * hit32).astype(BF)
    tok_c = tok_v[:, cols]
    zr_r[zc] = dot(d_logits, tok_c, TN)

    def zdev(off):
        return {"ep": lax.rem(zc + off, NZ) * NX + xc}

    def zsend(d):
        return remote(zr_r.at[zc], zr_r.at[zc], z_send, z_recv, zdev(d))

    each(1, NZ, lambda d: zsend(d).start())

    mark('gradsL')
    each(done, NY, grads)
    mark('rownorm')

    def rowd(k):
        return remote(row_v.at[k], rowd_r, rd_send, rd_recv, partner)

    rowd(1 - c).start()

    rd_wait = rowd(1 - c)

    router_back = dot(d_logits, rw_v[:, cols])

    mark('rdwait')
    rd_wait.wait_recv()
    rowy_r[y] = row_v[c] + rowd_r[...]

    def ry(d):
        return remote(rowy_r.at[y], rowy_r.at[y], ry_send, ry_recv, ydev(d))

    each(1, NY, lambda d: ry(d).start())

    mark('retwait')
    settle(ret_r.at[pl.ds(0, EP - 1)], ret_recv)
    mark('combine')
    back = dot(sel_v[...], ret_r[...].reshape(SLOTS, CW))
    tg_r[y, c] = (back + router_back).astype(BF)

    def tg(d):
        blk = tg_r.at[y, c]
        return remote(blk, blk, t_send, t_recv.at[y], ydev(d))

    def tg_wait(d):
        blk = tg_r.at[at(d), c]
        remote(blk, blk, t_send, t_recv.at[at(d)], ydev(d)).wait_recv()

    def tgd(src):
        blk = tg_r.at[src, c]
        return remote(blk, blk, td_send, td_recv, partner)

    each(0, NY - 1, lambda k: tg(y_order(k)).start())
    tgd(y).start()

    mark('zwait')
    settle(zr_r.at[pl.ds(0, NZ - 1)], z_recv)
    z_tot = zr_r[0]
    for j in range(1, NZ):
        z_tot = z_tot + zr_r[j]
    xr_r[xc] = z_tot

    def xdev(off):
        return {"ep": zc * NX + lax.rem(xc + off, NX)}

    def xsend(d):
        return remote(xr_r.at[xc], xr_r.at[xc], x_send, x_recv, xdev(d))

    each(1, NX, lambda d: xsend(d).start())
    mark('rywait')
    settle(rowy_r.at[pl.ds(0, NY - 1)], ry_recv)
    r_tot = rowy_r[0]
    for j in range(1, NY):
        r_tot = r_tot + rowy_r[j]
    rowf_s[c] = r_tot
    rf = remote(rowf_s.at[c], rowf_s.at[c], rf_send, rf_recv, partner)
    rf.start()
    mark('down')
    drow_o[...] = jnp.zeros_like(drow_o)
    each(0, NY, down_grads)
    mark('xwait')
    if NX > 1:
        settle(xr_r.at[pl.ds(0, NX - 1)], x_recv)
    x_tot = xr_r[0]
    for j in range(1, NX):
        x_tot = x_tot + xr_r[j]
    rg_o[...] = x_tot
    rr_o[...] = jnp.sum(x_tot * x_tot, axis=0, keepdims=True)

    mark('drain')
    for k in range(6):
        settle(a_s.at[k, pl.ds(0, EP - 1)], a_send.at[k])
    settle(g_s.at[pl.ds(0, EP - 1)], g_send)
    settle(ret_s.at[pl.ds(0, EP - 1)], ret_send)
    settle(gf_r.at[pl.ds(0, TP - 1)], gf_send)
    settle(zr_r.at[pl.ds(0, NZ - 1)], z_send)
    if NX > 1:
        settle(xr_r.at[pl.ds(0, NX - 1)], x_send)
    settle(rowy_r.at[pl.ds(0, NY - 1)], ry_send)
    settle(xa, d_send)
    settle(xa.at[pl.ds(0, 2 * H - 3)], y_send)
    settle(rs_s.at[pl.ds(0, 2 * H - 1)], rs_send)
    cp_w.wait_send()
    for h in (0, 1):
        cp_gp(h).wait_send()
    rd_wait.wait_send()
    remote(rowf_s.at[1 - c], rowf_s.at[1 - c], rf_send, rf_recv, partner).wait_recv()
    rf.wait_send()

    mark('agwait')

    def arrive(k):
        d = y_order(NY - 2 - k)
        tg_wait(d)
        tgd(at(d)).start()

    each(0, NY - 1, arrive)
    mark('agd')
    settle(tg_r.at[pl.ds(0, NY - 1), c], t_send)
    settle(tg_r.at[:, 1 - c], td_recv)
    settle(tg_r.at[:, c], td_send)
    mark(None)


def place(ny, tg, rg, rr, gg, ug, dg, rows, drow, tg_o, rg_o, rr_o, gg_o, ug_o, dg_o, gr_o, ur_o, drow_o, sem):
    pairs = [(gg, gg_o.at[0]), (ug, ug_o.at[0]), (dg, dg_o.at[0]), (rg, rg_o), (rr, rr_o),
             (rows.at[0], gr_o), (rows.at[1], ur_o), (drow, drow_o)]
    for j in range(ny):
        for k in (0, 1):
            pairs.append((tg.at[j, k], tg_o.at[:, pl.ds((2 * j + k) * CW, CW)]))
    copies = [pltpu.make_async_copy(a, b, sem.at[i]) for i, (a, b) in enumerate(pairs)]
    for cp in copies:
        cp.start()
    for cp in copies:
        cp.wait()


def build(ep, nx, ny, tok, width, cap):
    pc = 1
    while pc <= cap:
        pc *= 2
    rows, slots, tp, half = ep * cap, ep * pc, 2 * ny, ny // 2
    ns = rows // SUB
    hb = width // CW
    nz = ep // nx
    cfg = (ep, nx, ny, tok, width, cap, pc)
    v = pltpu.VMEM
    dma = pltpu.SemaphoreType.DMA
    scratch = [
        v((2, tok), jnp.int32), v((ep, width), BF),
        v((tok, width), BF), v((tok, width), BF), v((2, width, CW), BF), v((2, width, CW), BF), v((CW, width), BF),
        v((tok, slots), BF), v((rows, slots), BF),
        v((6, ep, pc, CW), BF), v((6, ep, pc, CW), BF),
        v((ny, 2, rows, CW), BF), v((ny, 2, rows, CW), BF),
        v((rows, CW), F32), v((rows, 2 * CW), F32), v((rows, CW), F32),
        v((rows, CW), BF), v((rows, 2 * CW), BF), v((rows, 2 * CW), BF), v((rows, CW), F32),
        v((2, rows, CW), F32), v((2 * half, rows, CW), BF), v((2 * half, rows, CW), BF),
        v((ep, pc, CW), BF), v((ep, pc, CW), BF),
        v((ep, 1, CW), F32), v((ep, 1, CW), F32), v((tp, 1, slots), F32),
        v((nz, ep, CW), F32), v((nx, ep, CW), F32),
        v((2, hb, 1, CW), F32), v((hb, 1, CW), F32), v((ny, hb, 1, CW), F32),
        dma((7,)), dma((6,)), dma((6,)), dma, dma((2, half, 2)), dma, dma((2, ny)), dma, dma, dma((2,)), dma((2,)),
        dma, dma, dma, dma, dma, dma((2, half, ns)), dma, dma, dma, dma, dma, dma, dma, dma, dma, dma, dma, dma,
        dma, dma((ny,)), dma, dma,
    ]
    sds = jax.ShapeDtypeStruct
    out_shape = (
        sds((ny, 2, tok, CW), BF), sds((ep, CW), F32), sds((1, CW), F32),
        sds((width, CW), BF), sds((width, CW), BF), sds((CW, width), BF),
        sds((2, hb, 1, CW), F32), sds((1, CW), F32),
    )
    vm = pl.BlockSpec(memory_space=pltpu.VMEM)
    hbm = pl.BlockSpec(memory_space=pltpu.HBM)
    anywhere = pl.BlockSpec(memory_space=pl.ANY)
    call = pl.pallas_call(
        functools.partial(kernel, cfg),
        out_shape=out_shape,
        in_specs=[hbm] * 7,
        out_specs=tuple([vm] * 8),
        scratch_shapes=scratch,
        compiler_params=pltpu.CompilerParams(
            collective_id=0, has_side_effects=True, vmem_limit_bytes=VMEM_MB * 1024 * 1024
        ),
        name="experts_backward",
    )
    finish = pl.pallas_call(
        functools.partial(place, ny),
        out_shape=(
            sds((tok, width), BF), sds((ep, CW), F32), sds((1, CW), F32),
            sds((1, width, CW), BF), sds((1, width, CW), BF), sds((1, CW, width), BF),
            sds((hb, 1, CW), F32), sds((hb, 1, CW), F32), sds((1, CW), F32),
        ),
        in_specs=[anywhere] * 8,
        out_specs=tuple([hbm] * 9),
        scratch_shapes=[dma((2 * ny + 8,))],
        compiler_params=pltpu.CompilerParams(vmem_limit_bytes=1024 * 1024),
        name="place_outputs",
    )

    def per_device(tokens, routing, router_weight, gate_weight, up_weight, down_weight, cotangent):
        args = (routing.T, router_weight.T, tokens, cotangent, gate_weight, up_weight, down_weight)
        parts = call(*[pltpu.with_memory_space_constraint(a, pltpu.HBM) for a in args])
        tg, rg, rr, gg, ug, dg, gr, ur, drow = finish(*parts)
        return (
            tg, rg.T, rr.reshape(CW), gg, ug, dg, gr.reshape(1, width), ur.reshape(1, width), drow,
        )

    return per_device


SPECS_IN = (
    P("ep", None), P("ep", None), P(), P("ep", None, "tp"), P("ep", None, "tp"), P("ep", "tp", None), P("ep", None),
)
SPECS_OUT = (
    P("ep", None), P("tp", None), P("tp"), P("ep", None, "tp"), P("ep", None, "tp"), P("ep", "tp", None),
    P("ep", None), P("ep", None), P("ep", "tp"),
)


def solution(mesh):
    ep, tp = mesh.shape["ep"], mesh.shape["tp"]
    body = build(ep, 4, tp // 2, 128, CW * tp, 14)
    return jax.shard_map(body, mesh=mesh, in_specs=SPECS_IN, out_specs=SPECS_OUT, check_vma=False)
```

time: 100 us -> 78 us (0.78)
  local copies, waits for them, and re-layouts: 11.5 us -> 0 us
  Pallas kernels: 87.6 us -> 77.2 us
    pallas_call x1 -> x2, Pallas kernels: 87.6 us -> 77.2 us  [the longest x1 75.7 us: per_device(): call(*[pltpu.with_memory_space_constraint(a, pltpu.HBM) for a in args])]
    unnamed x20 -> x0, local copies, waits for them, and re-layouts: 9.7 us -> none
    slice x1 -> x0, local copies, waits for them, and re-layouts: 1.2 us -> none  [per_device(): drow[0:1]]
where the time goes in v2:
time: 78 us; the launch traced here: 77.9 us
  Pallas kernels  77.2 us (99%)
    pallas_call x1, Pallas kernels, per_device(): call(*[pltpu.with_memory_space_constraint(a, pltpu.HBM) for a in args])  75.7 us

profile of v2, /device:TPU:1, one launch (start us, length us, event | category | flops | bytes accessed | tf_op | source)
XLA Modules:
  0.0 77.9 jit_solution(856594701154818701)
XLA Ops:
  0.6 75.7 %experts_backward.1 = (bf16[8,2,128,128]{3,2,1,0:T(8,128)(2,1)S(1)}, f32[32,128]{1,0:T(8,128)S(1)}, f32[1,128]{1,0:T(1,128)S(1)}, bf16[2048,128]{1,0:T(8,128)(2,...) custom-call(s32[2,128]{1,0:T(2,128)} %bitcast.7, ...), custom_call_target="tpu_custom_call" | custom-call | tf_op jit(solution)/shard_map/experts_backward/pallas_call | solution.py:659
  76.3 1.5 %place_outputs.1 = (bf16[128,2048]{1,0:T(8,128)(2,1)}, f32[32,128]{1,0:T(8,128)}, f32[1,128]{1,0:T(1,128)}, bf16[1,2048,128]{2,1,0:T(8,128)(2,1)}, bf16[1,2048,1...) custom-call(bf16[8,2,128,128]{3,2,1,0:T(8,128)(2,1)S(1)} %get-tuple-, ...), custom_call_target="tpu_custom_call" | custom-call | tf_op jit(solution)/shard_map/place_outputs/pallas_call | solution.py:660

commit v3 on v2

--- a/solution.py
+++ b/solution.py
@@ -36,12 +36,12 @@
     tg_r, rg_o, rr_o, gg_o, ug_o, dg_o, rowf_s, drow_o,
     rt_v, rw_v, tok_v, cot_v, w_own, w_par, dn_v,
     sel_v, cmp_v, a_s, a_r, xa, za, wcol, acc_gu, acc_b,
-    hid_v, gp_own, gp_par, tm_v, part_v, rs_s, rs_r, ret_s, ret_r,
-    g_s, g_r, gf_r, zr_r, xr_r, row_v, rowd_r, rowy_r,
+    hid_v, gp_own, gp_par, tm_v, part_v, own_v, rs_s, rs_r, ret_s, ret_r,
+    g_s, g_r, gf_r, zr_s, zr_r, xr_r, row_v, rowd_r, rowy_r, e_s, e_r, fw_s, fw_r,
     ld_sem, a_send, a_recv, y_send, y_recv, d_send, d_recv, w_send, w_recv, gp_send, gp_recv,
     g_send, g_recv, gf_send, gf_recv, rs_send, rs_recv, ret_send, ret_recv,
     z_send, z_recv, x_send, x_recv, rd_send, rd_recv, ry_send, ry_recv, rf_send, rf_recv,
-    t_send, t_recv, td_send, td_recv,
+    t_send, t_recv, td_send, td_recv, e_send, e_recv, fw_send, fw_recv,
 ):
     EP, NX, NY, T, D, CAP, PC = cfg
     cur = [None]
@@ -68,10 +68,20 @@
     c = lax.rem(tp, 2)
     zc = lax.div(ep, NX)
     xc = lax.rem(ep, NX)
-    partner = {"tp": y * 2 + (1 - c)}
+    other = 1 - c
+    partner = {"tp": y * 2 + other}
 
     def ydev(off):
         return {"tp": lax.rem(y + off + NY, NY) * 2 + c}
+
+    def ydev_x(off):
+        return {"tp": lax.rem(y + off + NY, NY) * 2 + other}
+
+    def home(peer):
+        return {"ep": peer, "tp": y * 2 + other}
+
+    def core_at(dist):
+        return other if dist % 2 else c
 
     def remote(src, dst, ss, rs, dev):
         return pltpu.make_async_remote_copy(
@@ -108,7 +118,14 @@
     def settle(ref, sem):
         pltpu.make_async_copy(ref, ref, sem).wait()
 
+    def each_home(body):
+        each_peer(body)
+        body(ep)
+
     def greet_ep(peer):
+        pl.semaphore_signal(barrier, inc=1, device_id=home(peer), device_id_type=pl.DeviceIdType.MESH)
+
+    def greet_x(peer):
         pl.semaphore_signal(barrier, inc=1, device_id={"ep": peer}, device_id_type=pl.DeviceIdType.MESH)
 
     def greet_tp(d):
@@ -116,6 +133,8 @@
                             device_id_type=pl.DeviceIdType.MESH)
 
     each_peer(greet_ep)
+    for x in xs_of[:-1]:
+        greet_x(zc * NX + x)
     each(1, TP, greet_tp)
     ld_rt = pltpu.make_async_copy(rt_h, rt_v, ld_sem.at[5])
     ld_rw = pltpu.make_async_copy(rw_h, rw_v, ld_sem.at[6])
@@ -163,10 +182,10 @@
         return lax.rem(y + off + NY, NY)
 
     def col_ds(chip):
-        return pl.ds(pl.multiple_of((chip * 2 + c) * CW, CW), CW)
-
-    cols = col_ds(y)
-    extra = ((0, y), (1, y), (0, at(H)), (1, at(H)), (0, at(H - 1)), (1, at(1 - H)))
+        return pl.ds(pl.multiple_of((chip * 2 + other) * CW, CW), CW)
+
+    cols_x = col_ds(y)
+    extra = ((0, y), (1, y), (0, at(H)), (1, at(H)), (1, at(H - 1)), (1, at(1 - H)))
     ld_cot.wait()
 
     def fill(k):
@@ -175,22 +194,25 @@
         if k == 0:
             val = val + dot(tail, w_rows.astype(BF))
         a_s[k] = val.astype(BF).reshape(EP, PC, CW)
-        a_r[k, ep] = a_s[k, ep]
 
     for k in range(6):
         fill(k)
     mark('barrier')
-    pl.semaphore_wait(barrier, EP - 1 + TP - 1)
+    pl.semaphore_wait(barrier, EP - 1 + NX - 1 + TP - 1)
 
     mark('a2a_issue')
 
     def a2a(k, peer):
-        return remote(a_s.at[k, peer], a_r.at[k, ep], a_send.at[k], a_recv.at[k], {"ep": peer})
-
-    each_peer(lambda p: a2a(0, p).start())
-    each_peer(lambda p: a2a(1, p).start())
+        used = pl.ds(0, CAP if k else PC)
+        return remote(a_s.at[k, peer, used], a_r.at[k, ep, used], a_send.at[k], a_recv.at[k], home(peer))
+
+    def filled(tiles):
+        return jnp.where(iota((EP, PC, CW), 1) < CAP, tiles, jnp.zeros_like(tiles)).reshape(SLOTS, CW)
+
+    each_home(lambda p: a2a(0, p).start())
+    each_home(lambda p: a2a(1, p).start())
     for k in range(2, 6):
-        each_peer(lambda p, k=k: a2a(k, p).start())
+        each_home(lambda p, k=k: a2a(k, p).start())
     ld_g.wait()
     ld_u.wait()
     ld_d.wait()
@@ -199,27 +221,26 @@
 
     bufs = (xa, za)
 
-    def hop(way, step, part, src):
-        blk = bufs[part].at[src, c]
-        return remote(blk, blk, y_send, y_recv.at[way, step - 1, part],
-                      ydev(1 if way == 0 else -1))
-
-    def cross(part, src):
-        blk = bufs[part].at[src, c]
+    def hop(way, step, part, src, sending=True):
+        blk = bufs[part].at[src, core_at(step - 1 if sending else step)]
+        return remote(blk, blk, y_send, y_recv.at[way, step - 1, part], ydev_x(1 if way == 0 else -1))
+
+    def cross(part, src, core):
+        blk = bufs[part].at[src, core]
         return remote(blk, blk, d_send, d_recv.at[part, src], partner)
 
     def cross_wait(part, src):
-        blk = bufs[part].at[src, 1 - c]
-        remote(blk, blk, d_send, d_recv.at[part, src], partner).wait_recv()
+        cross(part, src, c).wait_recv()
 
     def parts_of(way, step):
-        return (0, 1) if step < H - 1 else ((0,) if way == 0 else (1,))
+        return (0, 1) if step < H - 1 else (0,)
 
     def take(k):
         kind, chip = extra[k]
-        settle(a_r.at[k, pl.ds(0, EP - 1)], a_recv.at[k])
-        bufs[kind][chip, c] = dot(cmp_v[...], a_r[k].reshape(SLOTS, CW)).astype(BF)
-        cross(kind, chip).start()
+        settle(a_r.at[k, :, pl.ds(0, CAP if k else PC)], a_recv.at[k])
+        tiles = filled(a_r[k]) if k else a_r[k].reshape(SLOTS, CW)
+        bufs[kind][chip, c] = dot(cmp_v[...], tiles).astype(BF)
+        cross(kind, chip, c).start()
 
     for k in (0, 1):
         mark(f'a2a_wait{k}')
@@ -245,41 +266,68 @@
     def chunk_ds(src):
         return pl.ds(pl.multiple_of(src * 2 * CW, 2 * CW), 2 * CW)
 
-    def forward_chunk(src):
+    def forward_x(src):
         cross_wait(0, src)
         xs = jnp.concatenate([xa[src, 0], xa[src, 1]], axis=1)
         ds = chunk_ds(src)
         wgu = jnp.concatenate([w_own[0, ds, :], w_own[1, ds, :]], axis=1)
         acc_gu[...] += dot(xs, wgu)
+
+    def forward_z(src):
         cross_wait(1, src)
         zs = jnp.concatenate([za[src, 0], za[src, 1]], axis=1)
-        acc_b[...] += dot(zs, dn_v[:, ds], NT)
+        acc_b[...] += dot(zs, dn_v[:, chunk_ds(src)], NT)
+
+    def forward_chunk(src):
+        forward_x(src)
+        forward_z(src)
+
+    def receive(s, part):
+        mark(f'gather{s}{part}')
+        for way in (0, 1):
+            if part in parts_of(way, s):
+                src = at(-s if way == 0 else s)
+                hop(way, s, part, src, False).wait_recv()
+                if s < H - 1 and part in parts_of(way, s + 1):
+                    hop(way, s + 1, part, src).start()
+                cross(part, src, core_at(s)).start()
+        mark(f'fwd{s}{part}')
+
+    def both(s, body):
+        each(0, 2, lambda i: body(at((2 * i - 1) * s)))
+
+    def extra_part(k):
+        mark(f'extra{k}')
+        take(k)
 
     mark('fwd0')
     each(0, 1, lambda i: forward_chunk(at(i)))
-    for s in range(1, H):
-        mark(f'gather{s}')
-        for part in (0, 1):
-            for way in (0, 1):
-                if part not in parts_of(way, s):
-                    continue
-                src = at(-s if way == 0 else s)
-                hop(way, s, part, src).wait_recv()
-                if s < H - 1 and part in parts_of(way, s + 1):
-                    hop(way, s + 1, part, src).start()
-                cross(part, src).start()
-        mark(f'fwd{s}')
-        if s < H - 1:
-            each(0, 2, lambda i, s=s: forward_chunk(at((2 * i - 1) * s)))
-        if s == max(1, H - 2):
-            mark('extra')
-            take(2)
-            take(3)
-            each(0, 1, lambda i: forward_chunk(at(H + i)))
-            take(4)
-            take(5)
-    mark('fwdL')
-    each(0, 2, lambda i: forward_chunk(at((2 * i - 1) * (H - 1))))
+    if H == 4:
+        receive(1, 0)
+        receive(1, 1)
+        both(1, forward_x)
+        extra_part(2)
+        receive(2, 0)
+        both(1, forward_z)
+        extra_part(3)
+        receive(2, 1)
+        both(2, forward_x)
+        each(0, 1, lambda i: forward_chunk(at(H + i)))
+        extra_part(4)
+        both(2, forward_z)
+        extra_part(5)
+        receive(3, 0)
+        both(3, forward_z)
+        both(3, forward_x)
+    else:
+        for k in range(2, 6):
+            extra_part(k)
+        each(0, 1, lambda i: forward_chunk(at(H + i)))
+        for s in range(1, H):
+            for part in (0, 1) if s < H - 1 else (0,):
+                receive(s, part)
+            both(s, forward_x)
+            both(s, forward_z)
 
     mark('pointwise')
     RB = 32 if ROWS % 64 == 0 and (ROWS // 2) % 32 == 0 else 16
@@ -307,64 +355,70 @@
         return remote(gp_own.at[ds], gp_par.at[ds], gp_send.at[h], gp_recv.at[h], partner)
 
     for h in (0, 1):
-        each(h * (HR // RB), (h + 1) * (HR // RB), pointwise)
+        lax.fori_loop(h * (HR // RB), (h + 1) * (HR // RB), lambda i, carry: (pointwise(i), carry)[1], 0, unroll=True)
         cp_gp(h).start()
 
     mark('gpwait')
-    def weight_rows(w_v, off):
-        ds = pl.ds(pl.multiple_of(at(off) * 2 * CW + c * CW, CW), CW)
+    def weight_rows(w_v, off, core):
+        ds = pl.ds(pl.multiple_of(at(off) * 2 * CW + core * CW, CW), CW)
         return jnp.concatenate([w_v[0, ds, :], w_v[1, ds, :]], axis=1)
 
-    def partial_for(off):
-        return dot(gp_own[...], weight_rows(w_own, off), NT) + dot(gp_par[...], weight_rows(w_par, off), NT)
-
-    def rs(way, step, i):
-        ds = pl.ds(i * SUB, SUB)
-        return remote(rs_s.at[way * H + step - 1, ds], rs_r.at[way * H + step - 1, ds],
-                      rs_send, rs_recv.at[way, step - 1, i],
-                      ydev(1 if way == 0 else -1))
-
-    def subs(way, step):
-        if step > 1:
-            return tuple(range(NS))
-        return tuple(range(NS // 2, NS)) if way == 0 else tuple(range(NS // 2))
-
-    own_first = dot(gp_own[...], weight_rows(w_own, H), NT)
+    K = H - 1
+
+    def pair_parts(off_a, off_b, core_a, core_b, own_only=False, rows=slice(None), prior=None):
+        def side(w_v):
+            return jnp.concatenate([weight_rows(w_v, off_a, core_a), weight_rows(w_v, off_b, core_b)], axis=0)
+
+        first = dot(gp_own[rows, :], side(w_own), NT) if prior is None else prior
+        return first if own_only else first + dot(gp_par[rows, :], side(w_par), NT)
+
+    PPS = NZ // NS
+
+    def sub_at(p):
+        off = NS // 2 + (p + 1) // 2 * (1 - 2 * (p % 2))
+        return lax.rem(lax.div(zc, PPS) + off, NS)
+
+    sub_ids = [sub_at(p) for p in range(NS)]
+    sub_ds = [pl.ds(pl.multiple_of(i * SUB, 16), SUB) for i in sub_ids]
+
+    def rs(way, step, p):
+        ds = sub_ds[p]
+        return remote(rs_s.at[way * K + step - 1, ds], rs_r.at[way * K + step - 1, ds],
+                      rs_send, rs_recv.at[way, step - 1, p],
+                      ydev_x(1 if way == 0 else -1))
+
+    own_first = pair_parts(K, -K, core_at(K), core_at(K), own_only=True)
     cp_w.wait_recv()
     for h in (0, 1):
-        way = 1 - h
-        ds = pl.ds(h * HR, HR)
         cp_gp(h).wait_recv()
-        val = own_first[h * HR:(h + 1) * HR] + dot(gp_par[ds, :], weight_rows(w_par, H), NT)
-        rs_s[way * H, ds] = val.astype(BF)
-        for i in subs(way, 1):
-            rs(way, 1, i).start()
+    first_pair = pair_parts(K, -K, core_at(K), core_at(K), prior=own_first).astype(BF)
+    for way in (0, 1):
+        rs_s[way * K] = first_pair[:, way * CW:(way + 1) * CW]
+    for p in range(NS):
+        for way in (0, 1):
+            rs(way, 1, p).start()
 
     def own_parts(step):
-        part_v[0] = partial_for(H - step + 1)
-        part_v[1] = partial_for(-(H - step + 1))
-
-    def rs_step(step):
-        have = [(i, w) for i in range(NS) for w in (0, 1)]
-        have.sort(key=lambda t: (t[0] in subs(t[1], step - 1)))
-        for i, w in have:
-            ds = pl.ds(i * SUB, SUB)
-            val = part_v[w, ds, :]
-            if i in subs(w, step - 1):
+        part_v[...] = pair_parts(K - step + 1, step - K - 1, core_at(K - step + 1), core_at(K - step + 1))
+
+    def rs_step(step, between):
+        for i in range(NS):
+            for w in (0, 1):
+                ds = sub_ds[i]
                 rs(w, step - 1, i).wait_recv()
-                val = val + rs_r[w * H + step - 2, ds, :].astype(F32)
-            rs_s[w * H + step - 1, ds, :] = val.astype(BF)
-            rs(w, step, i).start()
+                val = part_v[ds, w * CW:(w + 1) * CW] + rs_r[w * K + step - 2, ds, :].astype(F32)
+                rs_s[w * K + step - 1, ds, :] = val.astype(BF)
+                rs(w, step, i).start()
+        between()
 
     mark('gterm')
     block_of = one_hot(((iota((EP, ROWS), 1) * inv) >> 16) == iota((EP, ROWS), 0), F32)
     g_s[...] = dot(block_of, tm_v[...], NN, HI).reshape(EP, 1, CW)
-    g_r[ep] = g_s[ep]
 
     def g_copy(peer, slot):
-        return remote(g_s.at[peer], g_r.at[slot], g_send, g_recv, {"ep": peer})
-
-    each_peer(lambda p: g_copy(p, ep).start())
+        return remote(g_s.at[peer], g_r.at[slot], g_send, g_recv, home(peer))
+
+    each_home(lambda p: g_copy(p, ep).start())
 
     ones = jnp.ones((8, 2 * CW), BF)
 
@@ -391,7 +445,7 @@
 
     def flatten_terms():
         mark('gflat')
-        settle(g_r.at[pl.ds(0, EP - 1)], g_recv)
+        settle(g_r, g_recv)
         lane_t = one_hot((iota((CW, SLOTS), 1) & (PC - 1)) == iota((CW, SLOTS), 0), F32)
         spread32 = one_hot((iota((EP, SLOTS), 1) >> shift) == iota((EP, SLOTS), 0), F32)
         g_flat = jnp.sum(dot(g_r[...].reshape(EP, CW), lane_t, NN, HI) * spread32, axis=0, keepdims=True)
@@ -406,45 +460,72 @@
         each(1, TP, lambda d: gf(tpeer(d), tp).start())
 
     mark('own2')
-    own_parts(2)
-    mark('rs2')
-    rs_step(2)
+    if K > 1:
+        own_parts(2)
+    mark('far')
+    far_near = pair_parts(H, 0, other, c)
+    own_v[...] = far_near[:, CW:]
+    e_s[...] = dot(cmp_v[...], far_near[:, :CW].astype(BF), TN).astype(BF).reshape(EP, PC, CW)
+
+    def far(peer):
+        used = pl.ds(0, CAP)
+        return remote(e_s.at[peer, used], e_r.at[ep, used], e_send, e_recv, home(peer))
+
+    each_home(lambda p: far(p).start())
     done = 0
-    for step in range(3, H + 1):
-        mark(f'own{step}')
-        own_parts(step)
-        each(done, done + 1, grads)
-        done += 1
+    for step in range(2, K + 1):
         mark(f'rs{step}')
-        rs_step(step)
-        if step == 3:
-            flatten_terms()
-    if H < 3:
-        flatten_terms()
-
+        rs_step(step, lambda: None)
+        if step < K:
+            mark(f'own{step + 1}')
+            own_parts(step + 1)
+            each(done, done + 1, grads)
+            done += 1
+    def far_home():
+        mark('farhome')
+        settle(e_r.at[:, pl.ds(0, CAP)], e_recv)
+        fw_s[...] = dot(sel_v[...], filled(e_r[...])).astype(BF)
+        cp_fw.start()
+
+    cp_fw = remote(fw_s, fw_r, fw_send, fw_recv, ydev_x(H))
+
+    flatten_terms()
     mark('rsfinal')
-    own = partial_for(0)
     BPS = SUB // CAP
 
     def ret(peer, slot):
-        return remote(ret_s.at[peer], ret_r.at[slot], ret_send, ret_recv, {"ep": peer})
-
-    for i in range(NS):
-        ds = pl.ds(i * SUB, SUB)
-        val = own[i * SUB:(i + 1) * SUB]
+        used = pl.ds(0, CAP)
+        return remote(ret_s.at[peer, used], ret_r.at[slot, used], ret_send, ret_recv, home(peer))
+
+    for p in range(NS):
+        mark(f'final{p}')
+        ds = sub_ds[p]
+        val = own_v[ds, :]
         for w in (0, 1):
-            rs(w, H, i).wait_recv()
-            val = val + rs_r[w * H + H - 1, ds, :].astype(F32)
-        spread_rows = cmp_v[ds, i * BPS * PC:(i + 1) * BPS * PC]
-        ret_s[i * BPS:(i + 1) * BPS] = dot(spread_rows, val.astype(BF), TN).astype(BF).reshape(BPS, PC, CW)
-
-        def send_back(b):
-            @pl.when(b != ep)
-            def _():
-                ret(b, ep).start()
-
-        each(i * BPS, (i + 1) * BPS, send_back)
-    ret_r[ep] = ret_s[ep]
+            rs(w, K, p).wait_recv()
+            val = val + rs_r[w * K + K - 1, ds, :].astype(F32)
+        first_block = sub_ids[p] * BPS
+        spread_rows = cmp_v[ds, pl.ds(pl.multiple_of(first_block * PC, 128), BPS * PC)]
+        ret_s[pl.ds(first_block, BPS)] = dot(spread_rows, val.astype(BF), TN).astype(BF).reshape(BPS, PC, CW)
+
+        def send_back(j, first_block=first_block):
+            ret(first_block + j, ep).start()
+
+        each(0, BPS, send_back)
+        if p == 1:
+            far_home()
+
+    mark('gradsL')
+    each(done, NY, grads)
+    mark('rownorm')
+    hb = D // CW
+
+    def rowd(k):
+        return remote(row_v.at[k], rowd_r, rd_send, rd_recv, partner)
+
+    rowd(1 - c).start()
+
+    rd_wait = rowd(1 - c)
 
     mark('router')
     settle(gf_r.at[pl.ds(0, TP - 1)], gf_recv)
@@ -456,33 +537,21 @@
         (iota((SLOTS, EP), 0) >> shift) == iota((SLOTS, EP), 1)))
     d_chosen = (d_w - jnp.sum(d_w * weights, axis=1, keepdims=True)) / total
     d_logits = (d_chosen * chosen * (1.0 - affinity) * hit32).astype(BF)
-    tok_c = tok_v[:, cols]
-    zr_r[zc] = dot(d_logits, tok_c, TN)
+    zr_s[...] = dot(d_logits, tok_v[:, cols_x], TN)
 
     def zdev(off):
-        return {"ep": lax.rem(zc + off, NZ) * NX + xc}
+        return home(lax.rem(zc + off, NZ) * NX + xc)
 
     def zsend(d):
-        return remote(zr_r.at[zc], zr_r.at[zc], z_send, z_recv, zdev(d))
-
-    each(1, NZ, lambda d: zsend(d).start())
-
-    mark('gradsL')
-    each(done, NY, grads)
-    mark('rownorm')
-
-    def rowd(k):
-        return remote(row_v.at[k], rowd_r, rd_send, rd_recv, partner)
-
-    rowd(1 - c).start()
-
-    rd_wait = rowd(1 - c)
-
-    router_back = dot(d_logits, rw_v[:, cols])
+        return remote(zr_s, zr_r.at[zc], z_send, z_recv, zdev(d))
+
+    each(0, NZ, lambda d: zsend(d).start())
+
+    router_back = dot(d_logits, rw_v[:, cols_x])
 
     mark('rdwait')
     rd_wait.wait_recv()
-    rowy_r[y] = row_v[c] + rowd_r[...]
+    rowy_r[y] = (row_v[c] + rowd_r[...]).reshape(hb, CW).astype(BF)
 
     def ry(d):
         return remote(rowy_r.at[y], rowy_r.at[y], ry_send, ry_recv, ydev(d))
@@ -490,28 +559,29 @@
     each(1, NY, lambda d: ry(d).start())
 
     mark('retwait')
-    settle(ret_r.at[pl.ds(0, EP - 1)], ret_recv)
+    settle(ret_r.at[:, pl.ds(0, CAP)], ret_recv)
     mark('combine')
-    back = dot(sel_v[...], ret_r[...].reshape(SLOTS, CW))
-    tg_r[y, c] = (back + router_back).astype(BF)
+    back = dot(sel_v[...], filled(ret_r[...]))
+    cp_fw.wait_recv()
+    tg_r[y, other] = (back + fw_r[...].astype(F32) + router_back).astype(BF)
 
     def tg(d):
-        blk = tg_r.at[y, c]
-        return remote(blk, blk, t_send, t_recv.at[y], ydev(d))
+        blk = tg_r.at[y, other]
+        return remote(blk, blk, t_send, t_recv.at[y], ydev_x(d))
 
     def tg_wait(d):
         blk = tg_r.at[at(d), c]
-        remote(blk, blk, t_send, t_recv.at[at(d)], ydev(d)).wait_recv()
-
-    def tgd(src):
-        blk = tg_r.at[src, c]
+        remote(blk, blk, t_send, t_recv.at[at(d)], ydev_x(d)).wait_recv()
+
+    def tgd(src, core):
+        blk = tg_r.at[src, core]
         return remote(blk, blk, td_send, td_recv, partner)
 
     each(0, NY - 1, lambda k: tg(y_order(k)).start())
-    tgd(y).start()
+    tgd(y, other).start()
 
     mark('zwait')
-    settle(zr_r.at[pl.ds(0, NZ - 1)], z_recv)
+    settle(zr_r, z_recv)
     z_tot = zr_r[0]
     for j in range(1, NZ):
         z_tot = z_tot + zr_r[j]
@@ -526,10 +596,10 @@
     each(1, NX, lambda d: xsend(d).start())
     mark('rywait')
     settle(rowy_r.at[pl.ds(0, NY - 1)], ry_recv)
-    r_tot = rowy_r[0]
+    r_tot = rowy_r[0].astype(F32)
     for j in range(1, NY):
-        r_tot = r_tot + rowy_r[j]
-    rowf_s[c] = r_tot
+        r_tot = r_tot + rowy_r[j].astype(F32)
+    rowf_s[c] = r_tot.reshape(hb, 1, CW)
     rf = remote(rowf_s.at[c], rowf_s.at[c], rf_send, rf_recv, partner)
     rf.start()
     mark('down')
@@ -546,17 +616,19 @@
 
     mark('drain')
     for k in range(6):
-        settle(a_s.at[k, pl.ds(0, EP - 1)], a_send.at[k])
-    settle(g_s.at[pl.ds(0, EP - 1)], g_send)
-    settle(ret_s.at[pl.ds(0, EP - 1)], ret_send)
+        settle(a_s.at[k, :, pl.ds(0, CAP if k else PC)], a_send.at[k])
+    settle(g_s, g_send)
+    settle(ret_s.at[:, pl.ds(0, CAP)], ret_send)
     settle(gf_r.at[pl.ds(0, TP - 1)], gf_send)
-    settle(zr_r.at[pl.ds(0, NZ - 1)], z_send)
+    settle(zr_r, z_send)
     if NX > 1:
         settle(xr_r.at[pl.ds(0, NX - 1)], x_send)
     settle(rowy_r.at[pl.ds(0, NY - 1)], ry_send)
     settle(xa, d_send)
     settle(xa.at[pl.ds(0, 2 * H - 3)], y_send)
-    settle(rs_s.at[pl.ds(0, 2 * H - 1)], rs_send)
+    settle(rs_s, rs_send)
+    settle(e_s.at[:, pl.ds(0, CAP)], e_send)
+    cp_fw.wait_send()
     cp_w.wait_send()
     for h in (0, 1):
         cp_gp(h).wait_send()
@@ -569,7 +641,7 @@
     def arrive(k):
         d = y_order(NY - 2 - k)
         tg_wait(d)
-        tgd(at(d)).start()
+        tgd(at(d), c).start()
 
     each(0, NY - 1, arrive)
     mark('agd')
@@ -611,14 +683,15 @@
         v((ny, 2, rows, CW), BF), v((ny, 2, rows, CW), BF),
         v((rows, CW), F32), v((rows, 2 * CW), F32), v((rows, CW), F32),
         v((rows, CW), BF), v((rows, 2 * CW), BF), v((rows, 2 * CW), BF), v((rows, CW), F32),
-        v((2, rows, CW), F32), v((2 * half, rows, CW), BF), v((2 * half, rows, CW), BF),
+        v((rows, 2 * CW), F32), v((rows, CW), F32), v((2 * half - 2, rows, CW), BF), v((2 * half - 2, rows, CW), BF),
         v((ep, pc, CW), BF), v((ep, pc, CW), BF),
         v((ep, 1, CW), F32), v((ep, 1, CW), F32), v((tp, 1, slots), F32),
-        v((nz, ep, CW), F32), v((nx, ep, CW), F32),
-        v((2, hb, 1, CW), F32), v((hb, 1, CW), F32), v((ny, hb, 1, CW), F32),
+        v((ep, CW), F32), v((nz, ep, CW), F32), v((nx, ep, CW), F32),
+        v((2, hb, 1, CW), F32), v((hb, 1, CW), F32), v((ny, hb, CW), BF),
+        v((ep, pc, CW), BF), v((ep, pc, CW), BF), v((tok, CW), BF), v((tok, CW), BF),
         dma((7,)), dma((6,)), dma((6,)), dma, dma((2, half, 2)), dma, dma((2, ny)), dma, dma, dma((2,)), dma((2,)),
-        dma, dma, dma, dma, dma, dma((2, half, ns)), dma, dma, dma, dma, dma, dma, dma, dma, dma, dma, dma, dma,
-        dma, dma((ny,)), dma, dma,
+        dma, dma, dma, dma, dma, dma((2, half - 1, ns)), dma, dma, dma, dma, dma, dma, dma, dma, dma, dma, dma, dma,
+        dma, dma((ny,)), dma, dma, dma, dma, dma, dma,
     ]
     sds = jax.ShapeDtypeStruct
     out_shape = (

time: 78 us -> 71.5 us (0.917)
  Pallas kernels: 77.2 us -> 70.7 us
    pallas_call x1, Pallas kernels: 75.7 us -> 69.1 us  [per_device(): call(*[pltpu.with_memory_space_constraint(a, pltpu.HBM) for a in args])]
where the time goes in v3:
time: 71.5 us; the launch traced here: 71.3 us
  Pallas kernels  70.7 us (99%)
    pallas_call x1, Pallas kernels, per_device(): call(*[pltpu.with_memory_space_constraint(a, pltpu.HBM) for a in args])  69.1 us
    pallas_call x1, Pallas kernels, per_device(): tg, rg, rr, gg, ug, dg, gr, ur, drow = finish(*parts)  1.53 us

profile of v3, /device:TPU:1, one launch (start us, length us, event | category | flops | bytes accessed | tf_op | source)
XLA Modules:
  0.0 71.3 jit_solution(9598600295219962276)
XLA Ops:
  0.6 69.1 %experts_backward.1 = (bf16[8,2,128,128]{3,2,1,0:T(8,128)(2,1)S(1)}, f32[32,128]{1,0:T(8,128)S(1)}, f32[1,128]{1,0:T(1,128)S(1)}, bf16[2048,128]{1,0:T(8,128)(2,...) custom-call(s32[2,128]{1,0:T(2,128)} %bitcast.7, ...), custom_call_target="tpu_custom_call" | custom-call | tf_op jit(solution)/shard_map/experts_backward/pallas_call | solution.py:732
  69.8 1.5 %place_outputs.1 = (bf16[128,2048]{1,0:T(8,128)(2,1)}, f32[32,128]{1,0:T(8,128)}, f32[1,128]{1,0:T(1,128)}, bf16[1,2048,128]{2,1,0:T(8,128)(2,1)}, bf16[1,2048,1...) custom-call(bf16[8,2,128,128]{3,2,1,0:T(8,128)(2,1)S(1)} %get-tuple-, ...), custom_call_target="tpu_custom_call" | custom-call | tf_op jit(solution)/shard_map/place_outputs/pallas_call | solution.py:733

commit v4 on v3

--- a/solution.py
+++ b/solution.py
@@ -10,16 +10,14 @@
 BF = jnp.bfloat16
 F32 = jnp.float32
 CW = 128
-SUB = 112
 VMEM_MB = 24
-HI = lax.Precision.HIGHEST
 NN = ((1,), (0,))
 NT = ((1,), (1,))
 TN = ((0,), (0,))
 
 
-def dot(a, b, dims=NN, precision=None):
-    return lax.dot_general(a, b, (dims, ((), ())), precision=precision, preferred_element_type=F32)
+def dot(a, b, dims=NN):
+    return lax.dot_general(a, b, (dims, ((), ())), preferred_element_type=F32)
 
 
 def iota(shape, dim):
@@ -59,7 +57,13 @@
     H = NY // 2
     ROWS = EP * CAP
     SLOTS = EP * PC
-    NS = ROWS // SUB
+    NS = min(4, NZ)
+    WK = 2
+    SUB = ROWS // NS
+    HR = ROWS // 2
+    HB = EP // 2
+    HS = SLOTS // 2
+    R0 = max(NZ // 4 - 1, 0)
     shift = PC.bit_length() - 1
     inv = 65536 // CAP + 1
     ep = lax.axis_index("ep")
@@ -118,9 +122,22 @@
     def settle(ref, sem):
         pltpu.make_async_copy(ref, ref, sem).wait()
 
-    def each_home(body):
-        each_peer(body)
-        body(ep)
+    near, far_half = (0, NZ // 2), (NZ // 2, NZ)
+    def to_experts(span, body):
+        def plane(q):
+            base = lax.rem(zc + R0 - q + NZ, NZ) * NX
+            for x in range(NX):
+                body(base + x, q * NX + xc)
+
+        each(span[0], span[1], plane)
+
+    def to_homes(span, body):
+        def plane(q):
+            base = lax.rem(zc + q - R0 + NZ, NZ) * NX
+            for x in range(NX):
+                body(base + x, q * NX + x)
+
+        each(span[0], span[1], plane)
 
     def greet_ep(peer):
         pl.semaphore_signal(barrier, inc=1, device_id=home(peer), device_id_type=pl.DeviceIdType.MESH)
@@ -191,7 +208,7 @@
     def fill(k):
         kind, chip = extra[k]
         val = dot(sel_b, (tok_v if kind == 0 else cot_v)[:, col_ds(chip)], TN)
-        if k == 0:
+        if k == WK:
             val = val + dot(tail, w_rows.astype(BF))
         a_s[k] = val.astype(BF).reshape(EP, PC, CW)
 
@@ -202,17 +219,23 @@
 
     mark('a2a_issue')
 
-    def a2a(k, peer):
-        used = pl.ds(0, CAP if k else PC)
-        return remote(a_s.at[k, peer, used], a_r.at[k, ep, used], a_send.at[k], a_recv.at[k], home(peer))
+    def a2a(k, h, peer, slot):
+        used = pl.ds(0, PC if k == WK else CAP)
+        return remote(a_s.at[k, peer, used], a_r.at[k, slot, used], a_send.at[k], a_recv.at[k, h], home(peer))
+
+    def dot_exact(picks, vals, dims=NN, swap=False):
+        hi = vals.astype(BF)
+        lo = (vals - hi.astype(F32)).astype(BF)
+        if swap:
+            return dot(hi, picks, dims) + dot(lo, picks, dims)
+        return dot(picks, hi, dims) + dot(picks, lo, dims)
 
     def filled(tiles):
-        return jnp.where(iota((EP, PC, CW), 1) < CAP, tiles, jnp.zeros_like(tiles)).reshape(SLOTS, CW)
-
-    each_home(lambda p: a2a(0, p).start())
-    each_home(lambda p: a2a(1, p).start())
-    for k in range(2, 6):
-        each_home(lambda p, k=k: a2a(k, p).start())
+        return jnp.where(iota(tiles.shape, 1) < CAP, tiles, jnp.zeros_like(tiles)).reshape(-1, CW)
+
+    for k in range(6):
+        for h, span in ((0, near), (1, far_half)) if k < 2 else ((1, far_half), (0, near)):
+            to_experts(span, lambda p, slot, k=k, h=h: a2a(k, h, p, slot).start())
     ld_g.wait()
     ld_u.wait()
     ld_d.wait()
@@ -221,45 +244,39 @@
 
     bufs = (xa, za)
 
-    def hop(way, step, part, src, sending=True):
-        blk = bufs[part].at[src, core_at(step - 1 if sending else step)]
-        return remote(blk, blk, y_send, y_recv.at[way, step - 1, part], ydev_x(1 if way == 0 else -1))
-
-    def cross(part, src, core):
-        blk = bufs[part].at[src, core]
+    def half_of(part, src, core, h):
+        return bufs[part].at[src, core, pl.ds(h * HR, HR)]
+
+    def hop(way, step, part, h, src, sending=True):
+        blk = half_of(part, src, core_at(step - 1 if sending else step), h)
+        return remote(blk, blk, y_send, y_recv.at[way, step - 1, part, h], ydev_x(1 if way == 0 else -1))
+
+    def cross(part, src, core, h):
+        blk = half_of(part, src, core, h)
         return remote(blk, blk, d_send, d_recv.at[part, src], partner)
 
     def cross_wait(part, src):
-        cross(part, src, c).wait_recv()
+        blk = bufs[part].at[src, c]
+        remote(blk, blk, d_send, d_recv.at[part, src], partner).wait_recv()
 
     def parts_of(way, step):
         return (0, 1) if step < H - 1 else (0,)
 
-    def take(k):
+    def take(k, h):
         kind, chip = extra[k]
-        settle(a_r.at[k, :, pl.ds(0, CAP if k else PC)], a_recv.at[k])
-        tiles = filled(a_r[k]) if k else a_r[k].reshape(SLOTS, CW)
-        bufs[kind][chip, c] = dot(cmp_v[...], tiles).astype(BF)
-        cross(kind, chip, c).start()
+        blocks = pl.ds(h * HB, HB)
+        settle(a_r.at[k, blocks, pl.ds(0, PC if k == WK else CAP)], a_recv.at[k, h])
+        tiles = a_r[k, blocks].reshape(HS, CW) if k == WK else filled(a_r[k, blocks])
+        bufs[kind][chip, c, h * HR:(h + 1) * HR] = dot(cmp_v[0:HR, 0:HS], tiles).astype(BF)
+        cross(kind, chip, c, h).start()
 
     for k in (0, 1):
-        mark(f'a2a_wait{k}')
-        take(k)
-        for way in (0, 1):
-            if k in parts_of(way, 1):
-                hop(way, 1, k, y).start()
-    rx_all = a_r[0].reshape(SLOTS, CW)
-
-    mark('wcol')
-    pick = one_hot(
-        iota((ROWS, SLOTS), 1) == (row_src * PC + CAP)
-    )
-    w_sel = dot(pick, rx_all)
-    r2 = iota((ROWS, CW), 0)
-    r2_pos = r2 - ((r2 * inv) >> 16) * CAP
-    w_masked = jnp.where(r2_pos == iota((ROWS, CW), 1), w_sel, 0.0)
-    wcol[...] = jnp.broadcast_to(jnp.sum(w_masked, axis=1, keepdims=True), (ROWS, CW))
-
+        for h in (0, 1):
+            mark(f'a2a_wait{k}{h}')
+            take(k, h)
+            for way in (0, 1):
+                if k in parts_of(way, 1):
+                    hop(way, 1, k, h, y).start()
     acc_gu[...] = jnp.zeros_like(acc_gu)
     acc_b[...] = jnp.zeros_like(acc_b)
 
@@ -284,13 +301,14 @@
 
     def receive(s, part):
         mark(f'gather{s}{part}')
-        for way in (0, 1):
-            if part in parts_of(way, s):
-                src = at(-s if way == 0 else s)
-                hop(way, s, part, src, False).wait_recv()
-                if s < H - 1 and part in parts_of(way, s + 1):
-                    hop(way, s + 1, part, src).start()
-                cross(part, src, core_at(s)).start()
+        for h in (0, 1):
+            for way in (0, 1):
+                if part in parts_of(way, s):
+                    src = at(-s if way == 0 else s)
+                    hop(way, s, part, h, src, False).wait_recv()
+                    if s < H - 1 and part in parts_of(way, s + 1):
+                        hop(way, s + 1, part, h, src).start()
+                    cross(part, src, core_at(s), h).start()
         mark(f'fwd{s}{part}')
 
     def both(s, body):
@@ -298,30 +316,44 @@
 
     def extra_part(k):
         mark(f'extra{k}')
-        take(k)
+        take(k, 0)
+        take(k, 1)
+
+    def slot_weights():
+        mark('wcol')
+        pick = one_hot(
+            iota((ROWS, SLOTS), 1) == (row_src * PC + CAP)
+        )
+        w_sel = dot(pick, a_r[WK].reshape(SLOTS, CW))
+        r2 = iota((ROWS, CW), 0)
+        r2_pos = r2 - ((r2 * inv) >> 16) * CAP
+        w_masked = jnp.where(r2_pos == iota((ROWS, CW), 1), w_sel, 0.0)
+        wcol[...] = jnp.broadcast_to(jnp.sum(w_masked, axis=1, keepdims=True), (ROWS, CW))
 
     mark('fwd0')
     each(0, 1, lambda i: forward_chunk(at(i)))
     if H == 4:
         receive(1, 0)
+        extra_part(2)
+        slot_weights()
         receive(1, 1)
         both(1, forward_x)
-        extra_part(2)
+        extra_part(3)
         receive(2, 0)
         both(1, forward_z)
-        extra_part(3)
+        each(0, 1, lambda i: forward_chunk(at(H + i)))
+        extra_part(4)
         receive(2, 1)
         both(2, forward_x)
-        each(0, 1, lambda i: forward_chunk(at(H + i)))
-        extra_part(4)
+        extra_part(5)
         both(2, forward_z)
-        extra_part(5)
         receive(3, 0)
         both(3, forward_z)
         both(3, forward_x)
     else:
         for k in range(2, 6):
             extra_part(k)
+        slot_weights()
         each(0, 1, lambda i: forward_chunk(at(H + i)))
         for s in range(1, H):
             for part in (0, 1) if s < H - 1 else (0,):
@@ -348,13 +380,11 @@
         gp_own[ds, :CW] = (sc * pu * s * (1.0 + pg * (1.0 - s))).astype(BF)
         gp_own[ds, CW:] = (sc * pg * s).astype(BF)
 
-    HR = ROWS // 2
-
     def cp_gp(h):
         ds = pl.ds(h * HR, HR)
         return remote(gp_own.at[ds], gp_par.at[ds], gp_send.at[h], gp_recv.at[h], partner)
 
-    for h in (0, 1):
+    for h in (1, 0):
         lax.fori_loop(h * (HR // RB), (h + 1) * (HR // RB), lambda i, carry: (pointwise(i), carry)[1], 0, unroll=True)
         cp_gp(h).start()
 
@@ -372,14 +402,8 @@
         first = dot(gp_own[rows, :], side(w_own), NT) if prior is None else prior
         return first if own_only else first + dot(gp_par[rows, :], side(w_par), NT)
 
-    PPS = NZ // NS
-
-    def sub_at(p):
-        off = NS // 2 + (p + 1) // 2 * (1 - 2 * (p % 2))
-        return lax.rem(lax.div(zc, PPS) + off, NS)
-
-    sub_ids = [sub_at(p) for p in range(NS)]
-    sub_ds = [pl.ds(pl.multiple_of(i * SUB, 16), SUB) for i in sub_ids]
+    sub_ids = [NS // 2] + list(range(NS // 2 + 1, NS)) + list(range(NS // 2 - 1, -1, -1))
+    sub_ds = [pl.ds(i * SUB, SUB) for i in sub_ids]
 
     def rs(way, step, p):
         ds = sub_ds[p]
@@ -389,14 +413,16 @@
 
     own_first = pair_parts(K, -K, core_at(K), core_at(K), own_only=True)
     cp_w.wait_recv()
-    for h in (0, 1):
+    for h in (1, 0):
         cp_gp(h).wait_recv()
-    first_pair = pair_parts(K, -K, core_at(K), core_at(K), prior=own_first).astype(BF)
-    for way in (0, 1):
-        rs_s[way * K] = first_pair[:, way * CW:(way + 1) * CW]
-    for p in range(NS):
+        lo = h * HR
+        pair = pair_parts(K, -K, core_at(K), core_at(K), rows=pl.ds(lo, HR), prior=own_first[lo:lo + HR]).astype(BF)
         for way in (0, 1):
-            rs(way, 1, p).start()
+            rs_s[way * K, pl.ds(lo, HR)] = pair[:, way * CW:(way + 1) * CW]
+        for p in range(NS):
+            if sub_ids[p] // (NS // 2) == h:
+                for way in (0, 1):
+                    rs(way, 1, p).start()
 
     def own_parts(step):
         part_v[...] = pair_parts(K - step + 1, step - K - 1, core_at(K - step + 1), core_at(K - step + 1))
@@ -412,13 +438,13 @@
         between()
 
     mark('gterm')
-    block_of = one_hot(((iota((EP, ROWS), 1) * inv) >> 16) == iota((EP, ROWS), 0), F32)
-    g_s[...] = dot(block_of, tm_v[...], NN, HI).reshape(EP, 1, CW)
+    block_of = one_hot(((iota((EP, ROWS), 1) * inv) >> 16) == iota((EP, ROWS), 0))
+    g_s[...] = dot_exact(block_of, tm_v[...]).reshape(EP, 1, CW)
 
     def g_copy(peer, slot):
-        return remote(g_s.at[peer], g_r.at[slot], g_send, g_recv, home(peer))
-
-    each_home(lambda p: g_copy(p, ep).start())
+        return remote(g_s.at[slot], g_r.at[ep], g_send, g_recv, home(peer))
+
+    to_homes((0, NZ), lambda p, slot: g_copy(p, slot).start())
 
     ones = jnp.ones((8, 2 * CW), BF)
 
@@ -446,9 +472,8 @@
     def flatten_terms():
         mark('gflat')
         settle(g_r, g_recv)
-        lane_t = one_hot((iota((CW, SLOTS), 1) & (PC - 1)) == iota((CW, SLOTS), 0), F32)
-        spread32 = one_hot((iota((EP, SLOTS), 1) >> shift) == iota((EP, SLOTS), 0), F32)
-        g_flat = jnp.sum(dot(g_r[...].reshape(EP, CW), lane_t, NN, HI) * spread32, axis=0, keepdims=True)
+        g_flat = jnp.sum(
+            dot_exact(lane_of, g_r[...].reshape(EP, CW), NT, swap=True) * spread.astype(F32), axis=0, keepdims=True)
         gf_r[tp] = g_flat
 
         def gf(peer, slot):
@@ -467,11 +492,11 @@
     own_v[...] = far_near[:, CW:]
     e_s[...] = dot(cmp_v[...], far_near[:, :CW].astype(BF), TN).astype(BF).reshape(EP, PC, CW)
 
-    def far(peer):
+    def far(peer, slot):
         used = pl.ds(0, CAP)
-        return remote(e_s.at[peer, used], e_r.at[ep, used], e_send, e_recv, home(peer))
-
-    each_home(lambda p: far(p).start())
+        return remote(e_s.at[slot, used], e_r.at[ep, used], e_send, e_recv, home(peer))
+
+    to_homes((0, NZ), lambda p, slot: far(p, slot).start())
     done = 0
     for step in range(2, K + 1):
         mark(f'rs{step}')
@@ -479,8 +504,6 @@
         if step < K:
             mark(f'own{step + 1}')
             own_parts(step + 1)
-            each(done, done + 1, grads)
-            done += 1
     def far_home():
         mark('farhome')
         settle(e_r.at[:, pl.ds(0, CAP)], e_recv)
@@ -495,7 +518,7 @@
 
     def ret(peer, slot):
         used = pl.ds(0, CAP)
-        return remote(ret_s.at[peer, used], ret_r.at[slot, used], ret_send, ret_recv, home(peer))
+        return remote(ret_s.at[slot, used], ret_r.at[ep, used], ret_send, ret_recv, home(peer))
 
     for p in range(NS):
         mark(f'final{p}')
@@ -505,13 +528,10 @@
             rs(w, K, p).wait_recv()
             val = val + rs_r[w * K + K - 1, ds, :].astype(F32)
         first_block = sub_ids[p] * BPS
-        spread_rows = cmp_v[ds, pl.ds(pl.multiple_of(first_block * PC, 128), BPS * PC)]
-        ret_s[pl.ds(first_block, BPS)] = dot(spread_rows, val.astype(BF), TN).astype(BF).reshape(BPS, PC, CW)
-
-        def send_back(j, first_block=first_block):
-            ret(first_block + j, ep).start()
-
-        each(0, BPS, send_back)
+        ret_s[first_block:first_block + BPS] = dot(
+            cmp_v[0:SUB, 0:BPS * PC], val.astype(BF), TN).astype(BF).reshape(BPS, PC, CW)
+        planes = BPS // NX
+        to_homes((sub_ids[p] * planes, (sub_ids[p] + 1) * planes), lambda b, slot: ret(b, slot).start())
         if p == 1:
             far_home()
 
@@ -537,7 +557,7 @@
         (iota((SLOTS, EP), 0) >> shift) == iota((SLOTS, EP), 1)))
     d_chosen = (d_w - jnp.sum(d_w * weights, axis=1, keepdims=True)) / total
     d_logits = (d_chosen * chosen * (1.0 - affinity) * hit32).astype(BF)
-    zr_s[...] = dot(d_logits, tok_v[:, cols_x], TN)
+    zr_s[...] = dot(d_logits, tok_v[:, cols_x], TN).astype(BF)
 
     def zdev(off):
         return home(lax.rem(zc + off, NZ) * NX + xc)
@@ -580,11 +600,14 @@
     each(0, NY - 1, lambda k: tg(y_order(k)).start())
     tgd(y, other).start()
 
+    mark('down')
+    drow_o[...] = jnp.zeros_like(drow_o)
+    each(0, NY, down_grads)
     mark('zwait')
     settle(zr_r, z_recv)
-    z_tot = zr_r[0]
+    z_tot = zr_r[0].astype(F32)
     for j in range(1, NZ):
-        z_tot = z_tot + zr_r[j]
+        z_tot = z_tot + zr_r[j].astype(F32)
     xr_r[xc] = z_tot
 
     def xdev(off):
@@ -602,27 +625,13 @@
     rowf_s[c] = r_tot.reshape(hb, 1, CW)
     rf = remote(rowf_s.at[c], rowf_s.at[c], rf_send, rf_recv, partner)
     rf.start()
-    mark('down')
-    drow_o[...] = jnp.zeros_like(drow_o)
-    each(0, NY, down_grads)
-    mark('xwait')
-    if NX > 1:
-        settle(xr_r.at[pl.ds(0, NX - 1)], x_recv)
-    x_tot = xr_r[0]
-    for j in range(1, NX):
-        x_tot = x_tot + xr_r[j]
-    rg_o[...] = x_tot
-    rr_o[...] = jnp.sum(x_tot * x_tot, axis=0, keepdims=True)
-
     mark('drain')
     for k in range(6):
-        settle(a_s.at[k, :, pl.ds(0, CAP if k else PC)], a_send.at[k])
+        settle(a_s.at[k, :, pl.ds(0, PC if k == WK else CAP)], a_send.at[k])
     settle(g_s, g_send)
     settle(ret_s.at[:, pl.ds(0, CAP)], ret_send)
     settle(gf_r.at[pl.ds(0, TP - 1)], gf_send)
     settle(zr_r, z_send)
-    if NX > 1:
-        settle(xr_r.at[pl.ds(0, NX - 1)], x_send)
     settle(rowy_r.at[pl.ds(0, NY - 1)], ry_send)
     settle(xa, d_send)
     settle(xa.at[pl.ds(0, 2 * H - 3)], y_send)
@@ -633,8 +642,6 @@
     for h in (0, 1):
         cp_gp(h).wait_send()
     rd_wait.wait_send()
-    remote(rowf_s.at[1 - c], rowf_s.at[1 - c], rf_send, rf_recv, partner).wait_recv()
-    rf.wait_send()
 
     mark('agwait')
 
@@ -644,7 +651,20 @@
         tgd(at(d), c).start()
 
     each(0, NY - 1, arrive)
+    mark('xwait')
+    if NX > 1:
+        settle(xr_r.at[pl.ds(0, NX - 1)], x_recv)
+    x_tot = xr_r[0]
+    for j in range(1, NX):
+        x_tot = x_tot + xr_r[j]
+    rg_o[...] = x_tot
+    rr_o[...] = jnp.sum(x_tot * x_tot, axis=0, keepdims=True)
+
     mark('agd')
+    if NX > 1:
+        settle(xr_r.at[pl.ds(0, NX - 1)], x_send)
+    remote(rowf_s.at[1 - c], rowf_s.at[1 - c], rf_send, rf_recv, partner).wait_recv()
+    rf.wait_send()
     settle(tg_r.at[pl.ds(0, NY - 1), c], t_send)
     settle(tg_r.at[:, 1 - c], td_recv)
     settle(tg_r.at[:, c], td_send)
@@ -669,7 +689,7 @@
     while pc <= cap:
         pc *= 2
     rows, slots, tp, half = ep * cap, ep * pc, 2 * ny, ny // 2
-    ns = rows // SUB
+    ns = min(4, ep // nx)
     hb = width // CW
     nz = ep // nx
     cfg = (ep, nx, ny, tok, width, cap, pc)
@@ -686,10 +706,10 @@
         v((rows, 2 * CW), F32), v((rows, CW), F32), v((2 * half - 2, rows, CW), BF), v((2 * half - 2, rows, CW), BF),
         v((ep, pc, CW), BF), v((ep, pc, CW), BF),
         v((ep, 1, CW), F32), v((ep, 1, CW), F32), v((tp, 1, slots), F32),
-        v((ep, CW), F32), v((nz, ep, CW), F32), v((nx, ep, CW), F32),
+        v((ep, CW), BF), v((nz, ep, CW), BF), v((nx, ep, CW), F32),
         v((2, hb, 1, CW), F32), v((hb, 1, CW), F32), v((ny, hb, CW), BF),
         v((ep, pc, CW), BF), v((ep, pc, CW), BF), v((tok, CW), BF), v((tok, CW), BF),
-        dma((7,)), dma((6,)), dma((6,)), dma, dma((2, half, 2)), dma, dma((2, ny)), dma, dma, dma((2,)), dma((2,)),
+        dma((7,)), dma((6,)), dma((6, 2)), dma, dma((2, half - 1, 2, 2)), dma, dma((2, ny)), dma, dma, dma((2,)), dma((2,)),
         dma, dma, dma, dma, dma, dma((2, half - 1, ns)), dma, dma, dma, dma, dma, dma, dma, dma, dma, dma, dma, dma,
         dma, dma((ny,)), dma, dma, dma, dma, dma, dma,
     ]

time: 71.5 us -> 68.9 us (0.964)
  Pallas kernels: 70.7 us -> 68.2 us
    pallas_call x1, Pallas kernels: 69.1 us -> 66.6 us  [per_device(): call(*[pltpu.with_memory_space_constraint(a, pltpu.HBM) for a in args])]
where the time goes in v4:
time: 68.9 us; the launch traced here: 68.8 us
  Pallas kernels  68.2 us (99%)
    pallas_call x1, Pallas kernels, per_device(): call(*[pltpu.with_memory_space_constraint(a, pltpu.HBM) for a in args])  66.6 us
    pallas_call x1, Pallas kernels, per_device(): tg, rg, rr, gg, ug, dg, gr, ur, drow = finish(*parts)  1.53 us

profile of v4, /device:TPU:1, one launch (start us, length us, event | category | flops | bytes accessed | tf_op | source)
XLA Modules:
  0.0 68.8 jit_solution(1882518777247334818)
XLA Ops:
  0.6 66.6 %experts_backward.1 = (bf16[8,2,128,128]{3,2,1,0:T(8,128)(2,1)S(1)}, f32[32,128]{1,0:T(8,128)S(1)}, f32[1,128]{1,0:T(1,128)S(1)}, bf16[2048,128]{1,0:T(8,128)(2,...) custom-call(s32[2,128]{1,0:T(2,128)} %bitcast.7, ...), custom_call_target="tpu_custom_call" | custom-call | tf_op jit(solution)/shard_map/experts_backward/pallas_call | solution.py:752
  67.3 1.5 %place_outputs.1 = (bf16[128,2048]{1,0:T(8,128)(2,1)}, f32[32,128]{1,0:T(8,128)}, f32[1,128]{1,0:T(1,128)}, bf16[1,2048,128]{2,1,0:T(8,128)(2,1)}, bf16[1,2048,1...) custom-call(bf16[8,2,128,128]{3,2,1,0:T(8,128)(2,1)S(1)} %get-tuple-, ...), custom_call_target="tpu_custom_call" | custom-call | tf_op jit(solution)/shard_map/place_outputs/pallas_call | solution.py:753

commit v5 on v4

--- a/solution.py
+++ b/solution.py
@@ -126,7 +126,7 @@
     def to_experts(span, body):
         def plane(q):
             base = lax.rem(zc + R0 - q + NZ, NZ) * NX
-            for x in range(NX):
+            for x in xs_of:
                 body(base + x, q * NX + xc)
 
         each(span[0], span[1], plane)
@@ -134,7 +134,7 @@
     def to_homes(span, body):
         def plane(q):
             base = lax.rem(zc + q - R0 + NZ, NZ) * NX
-            for x in range(NX):
+            for x in xs_of:
                 body(base + x, q * NX + x)
 
         each(span[0], span[1], plane)
@@ -497,7 +497,8 @@
         return remote(e_s.at[slot, used], e_r.at[ep, used], e_send, e_recv, home(peer))
 
     to_homes((0, NZ), lambda p, slot: far(p, slot).start())
-    done = 0
+    each(0, 1, grads)
+    done = 1
     for step in range(2, K + 1):
         mark(f'rs{step}')
         rs_step(step, lambda: None)

time: 68.9 us -> 68.2 us (0.990)
  Pallas kernels: 68.2 us -> 67.4 us
    pallas_call x1, Pallas kernels: 66.6 us -> 65.9 us  [per_device(): call(*[pltpu.with_memory_space_constraint(a, pltpu.HBM) for a in args])]
where the time goes in v5:
time: 68.2 us; the launch traced here: 68.1 us
  Pallas kernels  67.4 us (99%)
    pallas_call x1, Pallas kernels, per_device(): call(*[pltpu.with_memory_space_constraint(a, pltpu.HBM) for a in args])  65.9 us
    pallas_call x1, Pallas kernels, per_device(): tg, rg, rr, gg, ug, dg, gr, ur, drow = finish(*parts)  1.53 us

profile of v5, /device:TPU:1, one launch (start us, length us, event | category | flops | bytes accessed | tf_op | source)
XLA Modules:
  0.0 68.1 jit_solution(13888443425516953278)
XLA Ops:
  0.6 65.9 %experts_backward.1 = (bf16[8,2,128,128]{3,2,1,0:T(8,128)(2,1)S(1)}, f32[32,128]{1,0:T(8,128)S(1)}, f32[1,128]{1,0:T(1,128)S(1)}, bf16[2048,128]{1,0:T(8,128)(2,...) custom-call(s32[2,128]{1,0:T(2,128)} %bitcast.7, ...), custom_call_target="tpu_custom_call" | custom-call | tf_op jit(solution)/shard_map/experts_backward/pallas_call | solution.py:753
  66.6 1.5 %place_outputs.1 = (bf16[128,2048]{1,0:T(8,128)(2,1)}, f32[32,128]{1,0:T(8,128)}, f32[1,128]{1,0:T(1,128)}, bf16[1,2048,128]{2,1,0:T(8,128)(2,1)}, bf16[1,2048,1...) custom-call(bf16[8,2,128,128]{3,2,1,0:T(8,128)(2,1)S(1)} %get-tuple-, ...), custom_call_target="tpu_custom_call" | custom-call | tf_op jit(solution)/shard_map/place_outputs/pallas_call | solution.py:754
